TPU v7x, 32 devices: a whole 2x2x4 slice. The times are simulated.
32 devices in a mesh: ep: 16 (over z, y, x), tp: 2 (over core).
Axes of the slice: x: 2, y: 2, z: 4, core: 2. Of those that a mesh axis runs over, the one named last changes fastest.
Arguments:
- tokens: bfloat16 [256, 2048], P('ep'), may hold values from -6 to 6
- lengths: int32 [256], P('ep'), may hold values from 1 to 1024, as said below
- attn_gain: float32 [2048], replicated, may hold values from 0.1 to 1.9
- w_query: bfloat16 [2048, 1024], P(None, 'tp'), may hold values from -0.125 to 0.125
- w_key: bfloat16 [2048, 128], P(None, 'tp'), may hold values from -0.125 to 0.125
- w_value: bfloat16 [2048, 128], P(None, 'tp'), may hold values from -0.125 to 0.125
- head_bias: float32 [16], P('tp'), may hold values from -7 to -2
- key_cache: bfloat16 [256, 2, 64, 1024], P('ep', 'tp'), may hold values from -6 to 6
- value_cache: bfloat16 [256, 2, 64, 1024], P('ep', 'tp'), may hold values from -6 to 6
- w_attn_out: bfloat16 [1024, 2048], P('tp'), may hold values from -0.1875 to 0.1875
- ffn_gain: float32 [2048], replicated, may hold values from 0.1 to 1.9
- w_router: bfloat16 [2048, 16], replicated, may hold values from -0.125 to 0.125
- routes: int32 [256, 6], P('ep'), may hold values from 0 to 15, all different within a row; in each aligned block of 16 rows (0 to 15, 16 to 31, ...) at most 12 rows name the same one
- w_dense_gate: bfloat16 [2048, 512], P('ep', 'tp'), may hold values from -0.125 to 0.125
- w_dense_up: bfloat16 [2048, 512], P('ep', 'tp'), may hold values from -0.125 to 0.125
- w_dense_down: bfloat16 [512, 2048], P('tp', 'ep'), may hold values from -0.25 to 0.25
- dense_mix: float32 [2048], replicated, may hold values from -0.125 to 0.125
- w_expert_gate: bfloat16 [16, 2048, 512], P('ep', None, 'tp'), may hold values from -0.125 to 0.125
- w_expert_up: bfloat16 [16, 2048, 512], P('ep', None, 'tp'), may hold values from -0.125 to 0.125
- w_expert_down: bfloat16 [16, 512, 2048], P('ep', 'tp'), may hold values from -0.25 to 0.25
Outputs:
- layer_out: bfloat16 [256, 2048], P('ep', 'tp')
- new_keys: bfloat16 [256, 128], P('ep', 'tp')
- new_values: bfloat16 [256, 128], P('ep', 'tp')
Inputs may be any that keep to these rules, and one draw needn't show every extreme that they name: `lengths`: every sequence holds between 1 and 1024 cached positions; in every draw some sequence holds exactly 1024. `routes`: each token names 6 different experts. Among the rows of one device no expert is named by more than 12 rows.
All inputs are finite; a program needn't handle non-finite values.
Results may differ from a plain program's by a relative error of at most 0.014.
Values may be sent and summed in bfloat16 or wider, within the bound.
A program may use at most 64 MiB of HBM per device.

v0:
```python
import functools

import jax
import jax.numpy as jnp
from jax import lax
from jax.experimental import pallas as pl
from jax.experimental.pallas import tpu as pltpu
from jax.sharding import PartitionSpec as P

MESH = pl.DeviceIdType.MESH


def whole_layer(
    n,
    group_size,
    tokens_ref,
    attn_gain_ref,
    lengths_ref,
    bias_ref,
    w_key_ref,
    w_value_ref,
    gain_ref,
    router_ref,
    routes_ref,
    mix_ref,
    dense_gate_ref,
    dense_up_ref,
    down_ref,
    w_query_hbm,
    w_out_hbm,
    w_gate_hbm,
    w_up_hbm,
    w_down_hbm,
    keys_hbm,
    values_hbm,
    out_ref,
    new_keys_ref,
    new_values_ref,
    w_query,
    w_out,
    w_gate,
    w_up,
    w_down,
    keys,
    values,
    load_sem,
    keys_sem,
    values_sem,
    query_ref,
    score_ref,
    read_ref,
    normed_ref,
    dense_gate_all,
    dense_up_all,
    down_all,
    attn_mine,
    attn_peer,
    res_ref,
    norm_all,
    part_send,
    part_recv,
    hidden_ref,
    dense_all,
    cols_send,
    cols_recv,
    other_ref,
    mine_ref,
    peer_ref,
    back_send,
    back_recv,
    pair_sems,
    dense_gate_sems,
    dense_up_sems,
    down_sems,
    norm_sems,
    pass_sems,
    part_sems,
    dense_sems,
    cols_send_sem,
    cols_recv_sem,
    back_sems,
):
    me = lax.axis_index("ep")
    core = lax.axis_index("tp")
    peer = 1 - core
    rows, model = tokens_ref.shape
    half = model // 2
    width = dense_gate_ref.shape[0]
    window = width * group_size
    place = me % group_size
    team = me // group_size
    teams = n // group_size
    first = team * window
    owner = first // half
    lane = pl.multiple_of(first % half, window)
    f32 = jnp.float32
    local_heads = bias_ref.shape[1]
    head_dim, cache_len = keys_hbm.shape[1:]
    span = 4

    def remote(source, target, send_sem, recv_sem, ep, tp):
        return pltpu.make_async_remote_copy(
            src_ref=source,
            dst_ref=target,
            send_sem=send_sem,
            recv_sem=recv_sem,
            device_id=(ep, tp),
            device_id_type=MESH,
        )

    pairs = (
        (w_query_hbm, w_query),
        (w_gate_hbm, w_gate),
        (w_up_hbm, w_up),
        (w_down_hbm, w_down),
        (w_out_hbm, w_out),
    )
    loads = [
        pltpu.make_async_copy(source, target, load_sem.at[i])
        for i, (source, target) in enumerate(pairs)
    ]

    def keys_load(c):
        block = pl.ds(c * span, span)
        return pltpu.make_async_copy(keys_hbm.at[block], keys.at[block], keys_sem.at[c])

    def values_load(c):
        block = pl.ds(c * span, span)
        return pltpu.make_async_copy(values_hbm.at[block], values.at[block], values_sem.at[c])

    loads[0].start()
    for c in range(rows // span):
        keys_load(c).start()
        values_load(c).start()
    for load in (loads[4], loads[1], loads[2], loads[3]):
        load.start()

    barrier = pltpu.get_barrier_semaphore()

    def greet(k, carry):
        other = lax.rem(me + k, n)
        pl.semaphore_signal(barrier, inc=1, device_id=(other, core), device_id_type=MESH)
        pl.semaphore_signal(barrier, inc=1, device_id=(other, peer), device_id_type=MESH)
        return carry

    lax.fori_loop(1, n, greet, 0)
    pl.semaphore_signal(barrier, inc=1, device_id=(me, peer), device_id_type=MESH)

    start = tokens_ref[...].astype(f32)
    normed_ref[...] = (
        start
        * lax.rsqrt(jnp.mean(start * start, axis=-1, keepdims=True) + 1e-06)
        * attn_gain_ref[...]
    ).astype(jnp.bfloat16)
    loads[0].wait()
    queries = jnp.dot(normed_ref[...], w_query[...], preferred_element_type=f32)
    queries = queries.astype(jnp.bfloat16).astype(f32)
    for h in range(local_heads):
        query_ref[:, h, :] = queries[:, h * head_dim : (h + 1) * head_dim]
    pl.semaphore_wait(barrier, 2 * n - 1)

    def team_copy(source, gathered, sems, origin, other):
        return remote(
            source,
            gathered.at[origin],
            sems.at[0, other],
            sems.at[1, origin],
            team * group_size + other,
            core,
        )

    def send_weights(k, carry):
        other = lax.rem(place + k, group_size)
        team_copy(dense_gate_ref, dense_gate_all, dense_gate_sems, place, other).start()
        team_copy(dense_up_ref, dense_up_all, dense_up_sems, place, other).start()
        team_copy(down_ref, down_all, down_sems, place, other).start()
        return carry

    lax.fori_loop(1, group_size, send_weights, 0)
    dense_gate_all[place] = dense_gate_ref[...]
    dense_up_all[place] = dense_up_ref[...]
    down_all[place] = down_ref[...]

    block_len = min(256, cache_len)
    after_mask = (
        lax.broadcasted_iota(jnp.int32, (block_len, block_len), 0)
        > lax.broadcasted_iota(jnp.int32, (block_len, block_len), 1)
    ).astype(jnp.bfloat16)
    position = lax.broadcasted_iota(jnp.int32, (span * local_heads, block_len), 1)

    head_row = lax.broadcasted_iota(jnp.int32, (local_heads, local_heads), 0)
    head_col = lax.broadcasted_iota(jnp.int32, (local_heads, local_heads), 1)
    bias = jnp.sum(jnp.where(head_row == head_col, bias_ref[...], 0.0), axis=1, keepdims=True)
    lines = span * local_heads
    line_seq = lax.broadcasted_iota(jnp.int32, (lines, rows), 0) // local_heads
    seq_lane = lax.broadcasted_iota(jnp.int32, (lines, rows), 1)
    lengths_row = lengths_ref[...].astype(f32)

    def attend(c, carry):
        keys_load(c).wait()
        for i in range(span):
            s = c * span + i
            score_ref[s] = (
                jnp.dot(query_ref[s].astype(jnp.bfloat16), keys[s], preferred_element_type=f32)
                * head_dim ** (-0.5)
                + bias
            )
        limits = jnp.sum(
            jnp.where(seq_lane == line_seq + c * span, lengths_row, 0.0), axis=1, keepdims=True
        ).astype(jnp.int32)
        later = jnp.zeros((lines, 1), f32)
        for first_pos in range(cache_len - block_len, -1, -block_len):
            columns = slice(first_pos, first_pos + block_len)
            scores = score_ref[pl.ds(c * span, span), :, columns].reshape(lines, block_len)
            visible = position + first_pos < limits
            keep = -(jnp.maximum(scores, 0.0) + jnp.log1p(jnp.exp(-jnp.abs(scores))))
            log_take = scores + keep
            keep = jnp.where(visible, keep, 0.0)
            top = keep.astype(jnp.bfloat16)
            rest = keep - top.astype(f32)
            middle = rest.astype(jnp.bfloat16)
            low = (rest - middle.astype(f32)).astype(jnp.bfloat16)
            sums = jnp.dot(
                jnp.concatenate([top, middle, low], axis=0),
                after_mask,
                preferred_element_type=f32,
            )
            after = sums[:lines] + sums[lines : 2 * lines] + sums[2 * lines :] + later
            later = later + jnp.sum(keep, axis=-1, keepdims=True)
            stick = jnp.where(visible, jnp.exp(log_take + after), 0.0)
            score_ref[pl.ds(c * span, span), :, columns] = stick.reshape(
                span, local_heads, block_len
            )
        values_load(c).wait()
        for i in range(span):
            s = c * span + i
            read_ref[s] = lax.dot_general(
                score_ref[s].astype(jnp.bfloat16),
                values[s],
                (((1,), (1,)), ((), ())),
                preferred_element_type=f32,
            )
        return carry

    lax.fori_loop(0, rows // span, attend, 0)
    heads_out = jnp.concatenate(
        [read_ref[:, h, :] for h in range(local_heads)], axis=1
    ).astype(jnp.bfloat16)
    loads[4].wait()
    attn_mine[...] = jnp.dot(heads_out, w_out[...], preferred_element_type=f32).astype(
        jnp.bfloat16
    )

    swap = remote(attn_mine, attn_peer, pair_sems.at[0], pair_sems.at[1], me, peer)
    swap.start()
    swap.wait()
    attn = attn_mine[...].astype(f32) + attn_peer[...].astype(f32)
    residual = (tokens_ref[...].astype(f32) + attn).astype(jnp.bfloat16)
    res_ref[...] = residual
    wide = residual.astype(f32)
    normed = (
        wide * lax.rsqrt(jnp.mean(wide * wide, axis=-1, keepdims=True) + 1e-06) * gain_ref[...]
    ).astype(jnp.bfloat16)
    norm_all[0, me] = normed[:, :half]
    norm_all[1, me] = normed[:, half:]

    def norm_copy(j, other):
        return remote(
            norm_all.at[core, j],
            norm_all.at[core, j],
            norm_sems.at[0, other],
            norm_sems.at[1, j],
            other,
            core,
        )

    def pass_copy(j, which):
        return remote(
            norm_all.at[which, j],
            norm_all.at[which, j],
            pass_sems.at[0, j],
            pass_sems.at[1, j],
            me,
            peer,
        )

    def send_norm(k, carry):
        norm_copy(me, lax.rem(me + k, n)).start()
        return carry

    lax.fori_loop(1, n, send_norm, 0)

    across = (((1,), (1,)), ((), ()))
    probs = jax.nn.sigmoid(
        lax.dot_general(router_ref[...], normed, across, preferred_element_type=f32)
    )
    expert_total = probs.shape[0]
    expert_row = lax.broadcasted_iota(jnp.int32, (expert_total, rows), 0)
    hits = jnp.zeros((expert_total, rows), f32)
    for k in range(routes_ref.shape[0]):
        hits = jnp.where(routes_ref[k : k + 1, :] == expert_row, 1.0, hits)
    picked = jnp.where(hits > 0.0, probs, 0.0)
    gates = (picked / jnp.sum(picked, axis=0, keepdims=True) * 2.5).T
    expert_index = lax.broadcasted_iota(jnp.int32, (rows, expert_total), 1)
    mix_gate = jax.nn.sigmoid(
        jnp.sum(normed.astype(f32) * mix_ref[...], axis=-1, keepdims=True)
    )

    for weight, target in ((w_key_ref, new_keys_ref), (w_value_ref, new_values_ref)):
        target[...] = lax.dot_general(
            normed_ref[...], weight[...], across, preferred_element_type=f32
        ).astype(jnp.bfloat16)

    def take_norm(k, carry):
        j = lax.rem(me + n - k, n)
        norm_copy(j, me).wait_recv()
        pass_copy(j, core).start()
        return carry

    lax.fori_loop(1, n, take_norm, 0)

    def take_pass(k, carry):
        pass_copy(lax.rem(me + n - k, n), peer).wait_recv()
        return carry

    lax.fori_loop(1, n, take_pass, 0)

    def part_copy(m, other):
        return remote(
            part_send.at[other],
            part_recv.at[m],
            part_sems.at[0, other],
            part_sems.at[1, m],
            other * group_size + place,
            core,
        )

    def back_copy(j, other):
        return remote(
            back_send.at[other],
            back_recv.at[j],
            back_sems.at[0, other],
            back_sems.at[1, j],
            other,
            core,
        )

    def dense_copy(m, other):
        return remote(
            dense_all.at[m],
            dense_all.at[m],
            dense_sems.at[0, other],
            dense_sems.at[1, m],
            other * group_size + place,
            core,
        )

    group = min(n, 16)
    groups = n // group
    block = group * rows

    def take_weights(k, carry):
        other = lax.rem(place + k, group_size)
        team_copy(dense_gate_ref, dense_gate_all, dense_gate_sems, other, place).wait_recv()
        team_copy(dense_up_ref, dense_up_all, dense_up_sems, other, place).wait_recv()
        team_copy(down_ref, down_all, down_sems, other, place).wait_recv()
        return carry

    lax.fori_loop(1, group_size, take_weights, 0)
    features = jnp.concatenate(
        [norm_all[owner, m * group_size + place, :, pl.ds(lane, window)] for m in range(teams)],
        axis=0,
    )
    hidden_cols = dense_gate_ref.shape[1]
    for gathered, columns in (
        (dense_gate_all, slice(0, hidden_cols)),
        (dense_up_all, slice(hidden_cols, 2 * hidden_cols)),
    ):
        value = jnp.dot(
            features, gathered[...].reshape(window, hidden_cols), preferred_element_type=f32
        )
        part_send[:, :, columns] = value.astype(jnp.bfloat16).reshape(teams, rows, hidden_cols)

    def send_part(k, carry):
        part_copy(team, lax.rem(team + k, teams)).start()
        return carry

    lax.fori_loop(1, teams, send_part, 0)

    loads[1].wait()
    loads[2].wait()

    def expert_first(c, carry):
        base = c * group
        low = norm_all[0, pl.ds(base, group)].reshape(block, half)
        high = norm_all[1, pl.ds(base, group)].reshape(block, half)
        gate_rows = jnp.dot(low, w_gate[:half], preferred_element_type=f32) + jnp.dot(
            high, w_gate[half:], preferred_element_type=f32
        )
        up_rows = jnp.dot(low, w_up[:half], preferred_element_type=f32) + jnp.dot(
            high, w_up[half:], preferred_element_type=f32
        )
        hidden_ref[pl.ds(c, 1)] = (jax.nn.silu(gate_rows) * up_rows).astype(jnp.bfloat16)[None]
        return carry

    lax.fori_loop(0, groups, expert_first, 0)

    def take_part(k, total):
        m = lax.rem(team + teams - k, teams)
        part_copy(m, team).wait_recv()
        return total + part_recv[m].astype(f32)

    paired = lax.fori_loop(1, teams, take_part, part_send[team].astype(f32))
    dense_all[team] = (jax.nn.silu(paired[:, :hidden_cols]) * paired[:, hidden_cols:]).astype(
        jnp.bfloat16
    )

    def send_dense(k, carry):
        dense_copy(team, lax.rem(team + k, teams)).start()
        return carry

    lax.fori_loop(1, teams, send_dense, 0)

    loads[3].wait()
    far = pl.ds(pl.multiple_of(peer * half, half), half)
    near = pl.ds(pl.multiple_of(core * half, half), half)

    def expert_far(c, carry):
        value = jnp.dot(hidden_ref[c], w_down[:, far], preferred_element_type=f32)
        other_ref[pl.ds(c * group, group)] = value.astype(jnp.bfloat16).reshape(group, rows, half)
        return carry

    lax.fori_loop(0, groups, expert_far, 0)
    trade = remote(other_ref, peer_ref, pair_sems.at[2], pair_sems.at[3], me, peer)
    trade.start()

    def expert_near(c, carry):
        value = jnp.dot(hidden_ref[c], w_down[:, near], preferred_element_type=f32)
        mine_ref[pl.ds(c * group, group)] = value.astype(jnp.bfloat16).reshape(group, rows, half)
        return carry

    lax.fori_loop(0, groups, expert_near, 0)
    trade.wait()

    def send_back(k, carry):
        other = lax.rem(me + k, n)
        total = mine_ref[other].astype(f32) + peer_ref[other].astype(f32)
        back_send[other] = total.astype(jnp.bfloat16)

        @pl.when(k > 0)
        def _():
            back_copy(me, other).start()

        return carry

    lax.fori_loop(0, n, send_back, 0)

    def take_dense(k, carry):
        dense_copy(lax.rem(team + teams - k, teams), team).wait_recv()
        return carry

    lax.fori_loop(1, teams, take_dense, 0)
    dense_rows = dense_all[...].reshape(teams * rows, hidden_cols)
    columns = [
        jnp.dot(dense_rows, down_all[q], preferred_element_type=f32) for q in range(group_size)
    ]
    cols_send[...] = (
        jnp.concatenate(columns, axis=1).astype(jnp.bfloat16).reshape(cols_send.shape)
    )

    def cols_copy(from_core, m, other, target):
        return remote(
            cols_send.at[other],
            cols_recv.at[from_core, m],
            cols_send_sem.at[other],
            cols_recv_sem.at[from_core, m],
            other * group_size + place,
            target,
        )

    def send_cols(k, carry):
        cols_copy(core, team, lax.rem(team + k, teams), owner).start()
        return carry

    lax.fori_loop(1, teams, send_cols, 0)

    @pl.when(owner == core)
    def _():
        cols_recv[core, team] = cols_send[team]

    @pl.when(owner != core)
    def _():
        cols_copy(core, team, team, peer).start()

    side = teams // 2

    def take_cols(k, carry):
        m = core * side + k

        @pl.when(m != team)
        def _():
            cols_copy(core, m, team, core).wait_recv()

        cols_copy(peer, m, team, core).wait_recv()
        return carry

    lax.fori_loop(0, side, take_cols, 0)
    dense = jnp.concatenate(
        [
            cols_recv[0, core * side + q].astype(f32) + cols_recv[1, core * side + q].astype(f32)
            for q in range(side)
        ],
        axis=1,
    )
    total = res_ref[:, near].astype(f32) + mix_gate * dense

    def take_back(k, total):
        j = lax.rem(me + n - k, n)

        @pl.when(k > 0)
        def _():
            back_copy(j, me).wait_recv()

        @pl.when(k == 0)
        def _():
            back_recv[me] = back_send[me]

        gate = jnp.sum(jnp.where(expert_index == j, gates, 0.0), axis=-1, keepdims=True)
        return total + gate * back_recv[j].astype(f32)

    out_ref[...] = lax.fori_loop(0, n, take_back, total).astype(jnp.bfloat16)

    def drain(k, carry):
        other = lax.rem(me + k, n)
        norm_copy(me, other).wait_send()
        pass_copy(other, core).wait_send()
        back_copy(me, other).wait_send()
        return carry

    lax.fori_loop(1, n, drain, 0)

    def drain_team(k, carry):
        other = lax.rem(place + k, group_size)
        team_copy(dense_gate_ref, dense_gate_all, dense_gate_sems, place, other).wait_send()
        team_copy(dense_up_ref, dense_up_all, dense_up_sems, place, other).wait_send()
        team_copy(down_ref, down_all, down_sems, place, other).wait_send()
        return carry

    lax.fori_loop(1, group_size, drain_team, 0)

    def drain_dense(k, carry):
        other = lax.rem(team + k, teams)
        part_copy(team, other).wait_send()
        dense_copy(team, other).wait_send()
        cols_copy(core, team, other, owner).wait_send()
        return carry

    lax.fori_loop(1, teams, drain_dense, 0)

    @pl.when(owner != core)
    def _():
        cols_copy(core, team, team, peer).wait_send()


def shards(
    n,
    tokens,
    lengths,
    attn_gain,
    w_query,
    w_key,
    w_value,
    head_bias,
    key_cache,
    value_cache,
    w_attn_out,
    ffn_gain,
    w_router,
    routes,
    w_dense_gate,
    w_dense_up,
    w_dense_down,
    dense_mix,
    w_expert_gate,
    w_expert_up,
    w_expert_down,
):
    rows, model = tokens.shape
    half = model // 2
    width, hidden_cols = w_dense_gate.shape
    group_size = min(n, max(4, 128 // width))
    teams = n // group_size
    window = width * group_size
    seq_count, local_kv, head_dim, cache_len = key_cache.shape
    local_heads = head_bias.shape[0]
    keys = key_cache.reshape(seq_count, head_dim, cache_len)
    values = value_cache.reshape(seq_count, head_dim, cache_len)
    w_gate, w_up, w_down = w_expert_gate[0], w_expert_up[0], w_expert_down[0]
    expert_hidden = w_gate.shape[1]
    bf16, f32 = jnp.bfloat16, jnp.float32
    block = min(n, 16) * rows
    vmem = pl.BlockSpec(memory_space=pltpu.VMEM)
    anywhere = pl.BlockSpec(memory_space=pltpu.HBM)
    dma = pltpu.SemaphoreType.DMA
    return pl.pallas_call(
        functools.partial(whole_layer, n, group_size),
        out_shape=(
            jax.ShapeDtypeStruct((rows, half), bf16),
            jax.ShapeDtypeStruct((rows, w_key.shape[1]), bf16),
            jax.ShapeDtypeStruct((rows, w_value.shape[1]), bf16),
        ),
        in_specs=[vmem] * 13 + [anywhere] * 7,
        out_specs=(vmem, vmem, vmem),
        scratch_shapes=[
            pltpu.VMEM(w_query.shape, bf16),
            pltpu.VMEM(w_attn_out.shape, bf16),
            pltpu.VMEM(w_gate.shape, bf16),
            pltpu.VMEM(w_up.shape, bf16),
            pltpu.VMEM(w_down.shape, bf16),
            pltpu.VMEM(keys.shape, bf16),
            pltpu.VMEM(values.shape, bf16),
            dma((5,)),
            dma((rows // 4,)),
            dma((rows // 4,)),
            pltpu.VMEM((rows, local_heads, head_dim), f32),
            pltpu.VMEM((rows, local_heads, cache_len), f32),
            pltpu.VMEM((rows, local_heads, head_dim), f32),
            pltpu.VMEM((rows, model), bf16),
            pltpu.VMEM((group_size, width, hidden_cols), bf16),
            pltpu.VMEM((group_size, width, hidden_cols), bf16),
            pltpu.VMEM((group_size, hidden_cols, width), bf16),
            pltpu.VMEM((rows, model), bf16),
            pltpu.VMEM((rows, model), bf16),
            pltpu.VMEM((rows, model), bf16),
            pltpu.VMEM((2, n, rows, half), bf16),
            pltpu.VMEM((teams, rows, 2 * hidden_cols), bf16),
            pltpu.VMEM((teams, rows, 2 * hidden_cols), bf16),
            pltpu.VMEM((n * rows // block, block, expert_hidden), bf16),
            pltpu.VMEM((teams, rows, hidden_cols), bf16),
            pltpu.VMEM((teams, rows, window), bf16),
            pltpu.VMEM((2, teams, rows, window), bf16),
            pltpu.VMEM((n, rows, half), bf16),
            pltpu.VMEM((n, rows, half), bf16),
            pltpu.VMEM((n, rows, half), bf16),
            pltpu.VMEM((n, rows, half), bf16),
            pltpu.VMEM((n, rows, half), bf16),
            dma((4,)),
            dma((2, group_size)),
            dma((2, group_size)),
            dma((2, group_size)),
            dma((2, n)),
            dma((2, n)),
            dma((2, teams)),
            dma((2, teams)),
            dma((teams,)),
            dma((2, teams)),
            dma((2, n)),
        ],
        compiler_params=pltpu.CompilerParams(
            collective_id=0, has_side_effects=True, vmem_limit_bytes=63 * 1024 * 1024
        ),
        name="whole_layer",
    )(
        tokens,
        attn_gain.reshape(1, model),
        lengths.reshape(1, seq_count),
        head_bias.reshape(1, local_heads),
        w_key.T,
        w_value.T,
        ffn_gain.reshape(1, model),
        w_router.T,
        routes.T,
        dense_mix.reshape(1, model),
        w_dense_gate,
        w_dense_up,
        w_dense_down,
        w_query,
        w_attn_out,
        w_gate,
        w_up,
        w_down,
        keys,
        values,
    )


def solution(mesh):
    return jax.shard_map(
        functools.partial(shards, mesh.shape["ep"]),
        mesh=mesh,
        in_specs=(
            P("ep", None),
            P("ep"),
            P(),
            P(None, "tp"),
            P(None, "tp"),
            P(None, "tp"),
            P("tp"),
            P("ep", "tp", None, None),
            P("ep", "tp", None, None),
            P("tp", None),
            P(),
            P(),
            P("ep", None),
            P("ep", "tp"),
            P("ep", "tp"),
            P("tp", "ep"),
            P(),
            P("ep", None, "tp"),
            P("ep", None, "tp"),
            P("ep", "tp", None),
        ),
        out_specs=(P("ep", "tp"), P("ep", "tp"), P("ep", "tp")),
        check_vma=False,
    )
```

profile of v0, /device:TPU:7, one launch (start us, length us, event | category | flops | bytes accessed | tf_op | source)
XLA Modules:
  0.0 54.3 jit_solution(3005432509352608028)
XLA Ops:
  0.6 49.8 %whole_layer.1 = (bf16[16,1024]{1,0:T(8,128)(2,1)}, bf16[16,64]{1,0:T(8,128)(2,1)}, bf16[16,64]{1,0:T(8,128)(2,1)}) custom-call(bf16[16,2048]{1,0:T(8,128)(2,1)} %tokens_ref.1, f32[1,2048]{1,0:T(1,128)} %bitcast.22, s32[1,16]{1,0:T(1,128)} %bitcast.26, f32[1,8]{1,0:T(1,128)} %bitcast.27, bf16[64,2048]{1,0:T(8,128)(2,1)} %bitcast.19, ...), custom_call_target="tpu_custom_call" | custom-call | tf_op jit(solution)/shard_map/whole_layer/pallas_call | solution.py:605
  50.4 1.4 %copy.26 = bf16[16,1024]{1,0:T(8,128)(2,1)} copy(bf16[16,1024]{1,0:T(8,128)(2,1)} %get-tuple-element.6) | data formatting | bytes 65536
  51.8 1.3 %copy.27 = bf16[16,64]{1,0:T(8,128)(2,1)} copy(bf16[16,64]{1,0:T(8,128)(2,1)} %get-tuple-element.7) | data formatting | bytes 4096
  53.1 1.3 %copy.28 = bf16[16,64]{1,0:T(8,128)(2,1)} copy(bf16[16,64]{1,0:T(8,128)(2,1)} %get-tuple-element.8) | data formatting | bytes 4096
where the time goes:
time: 54.6 us; the launch traced here: 54.3 us
  Pallas kernels  49.8 us (91%)
  local copies, waits for them, and re-layouts  3.91 us (7%)
  between operations  0.65 us (1%)
    pallas_call x1, Pallas kernels, shards(): pl.pallas_call(functools.partial(whole_layer, n, group_size), out_shape=(...  49.8 us
    unnamed x3, local copies, waits for them, and re-layouts  3.91 us

commit v1 on v0

--- a/solution.py
+++ b/solution.py
@@ -562,6 +562,698 @@
         cols_copy(core, team, team, peer).wait_send()
 
 
+def flip(place, k):
+    result, bit = place, 1
+    while bit <= k:
+        if k & bit:
+            result = result + bit * (1 - 2 * ((place // bit) % 2))
+        bit *= 2
+    return result
+
+
+def routed_layer(
+    n,
+    inner,
+    tokens_hbm,
+    attn_gain_hbm,
+    lengths_hbm,
+    bias_hbm,
+    w_key_hbm,
+    w_value_hbm,
+    gain_hbm,
+    router_hbm,
+    routes_hbm,
+    mix_hbm,
+    dense_gate_hbm,
+    dense_up_hbm,
+    down_hbm,
+    w_query_hbm,
+    w_out_hbm,
+    w_gate_hbm,
+    w_up_hbm,
+    w_down_hbm,
+    keys_hbm,
+    values_hbm,
+    out_ref,
+    new_keys_ref,
+    new_values_ref,
+    tokens_ref,
+    attn_gain_ref,
+    lengths_ref,
+    bias_ref,
+    w_key_ref,
+    w_value_ref,
+    gain_ref,
+    router_ref,
+    routes_ref,
+    mix_ref,
+    dense_gate_ref,
+    dense_up_ref,
+    down_ref,
+    w_query,
+    w_out,
+    w_gate,
+    w_up,
+    w_down,
+    keys,
+    values,
+    query_ref,
+    score_ref,
+    read_ref,
+    normed_ref,
+    small_send,
+    small,
+    hits_all,
+    attn_mine,
+    attn_peer,
+    res_ref,
+    norm_all,
+    first_send,
+    first_recv,
+    plane_send,
+    plane_recv,
+    line_send,
+    line_recv,
+    load_sem,
+    keys_sem,
+    values_sem,
+    pair_sems,
+    swap_sems,
+    small_send_sem,
+    small_recv_sem,
+    down_send_sem,
+    down_recv_sem,
+    hits_sems,
+    line_sems,
+    spread_sems,
+    first_sems,
+    plane_sems,
+    back_sems,
+):
+    me = lax.axis_index("ep")
+    core = lax.axis_index("tp")
+    peer = 1 - core
+    f32, bf16 = jnp.float32, jnp.bfloat16
+    rows, model = tokens_ref.shape
+    half = model // 2
+    width, hidden_cols = dense_gate_ref.shape
+    units = hidden_cols // n
+    outer = n // inner
+    z, p = me // inner, me % inner
+    side = n // 2
+    owner, slot = me // side, me % side
+    local_heads = bias_ref.shape[1]
+    head_dim, cache_len = keys_hbm.shape[1:]
+    hidden = w_gate_hbm.shape[1]
+    expert_total = router_ref.shape[0]
+    lanes = small.shape[0]
+    router_at = 4 * units
+    mix_at = router_at + expert_total
+    span = 4
+    lines = span * local_heads
+
+    def remote(source, target, send_sem, recv_sem, ep, tp):
+        return pltpu.make_async_remote_copy(
+            src_ref=source,
+            dst_ref=target,
+            send_sem=send_sem,
+            recv_sem=recv_sem,
+            device_id=(ep, tp),
+            device_id_type=MESH,
+        )
+
+    near = pl.ds(pl.multiple_of(core * half, half), half)
+    far = pl.ds(pl.multiple_of(peer * half, half), half)
+    mine = pl.ds(pl.multiple_of(core * hidden, hidden), hidden)
+    pairs = (
+        (tokens_hbm, tokens_ref),
+        (attn_gain_hbm, attn_gain_ref),
+        (dense_gate_hbm, dense_gate_ref),
+        (dense_up_hbm, dense_up_ref),
+        (routes_hbm, routes_ref),
+        (w_query_hbm, w_query),
+        (bias_hbm, bias_ref),
+        (lengths_hbm, lengths_ref),
+        (router_hbm, router_ref),
+        (mix_hbm, mix_ref),
+        (down_hbm, down_ref),
+        (gain_hbm, gain_ref),
+        (w_out_hbm, w_out),
+        (w_key_hbm, w_key_ref),
+        (w_value_hbm, w_value_ref),
+        (w_gate_hbm.at[near, :], w_gate.at[:, mine]),
+        (w_up_hbm.at[near, :], w_up.at[:, mine]),
+        (w_down_hbm.at[:, near], w_down.at[mine, :]),
+    )
+    loads = [
+        pltpu.make_async_copy(source, target, load_sem.at[i])
+        for i, (source, target) in enumerate(pairs)
+    ]
+    load_of = {id(target): load for (_, target), load in zip(pairs, loads)}
+
+    def arrived(*targets):
+        for target in targets:
+            load_of[id(target)].wait()
+
+    def keys_load(c):
+        block = pl.ds(c * span, span)
+        return pltpu.make_async_copy(keys_hbm.at[block], keys.at[block], keys_sem.at[c])
+
+    def values_load(c):
+        block = pl.ds(c * span, span)
+        return pltpu.make_async_copy(values_hbm.at[block], values.at[block], values_sem.at[c])
+
+    for load in loads[:8]:
+        load.start()
+    for c in range(rows // span):
+        keys_load(c).start()
+        values_load(c).start()
+    for load in loads[8:]:
+        load.start()
+
+    barrier = pltpu.get_barrier_semaphore()
+
+    def greet(k, carry):
+        other = lax.rem(me + k, n)
+        pl.semaphore_signal(barrier, inc=1, device_id=(other, core), device_id_type=MESH)
+        pl.semaphore_signal(barrier, inc=1, device_id=(other, peer), device_id_type=MESH)
+        return carry
+
+    lax.fori_loop(1, n, greet, 0)
+    pl.semaphore_signal(barrier, inc=1, device_id=(me, peer), device_id_type=MESH)
+
+    arrived(tokens_ref, attn_gain_ref)
+    start = tokens_ref[...].astype(f32)
+    normed_ref[...] = (
+        start
+        * lax.rsqrt(jnp.mean(start * start, axis=-1, keepdims=True) + 1e-06)
+        * attn_gain_ref[...]
+    ).astype(bf16)
+    arrived(dense_gate_ref, dense_up_ref, routes_ref)
+    small_send[:, :units, :] = dense_gate_ref[...].T.reshape(n, units, width)
+    small_send[:, units:, :] = dense_up_ref[...].T.reshape(n, units, width)
+    lane_row = lax.broadcasted_iota(jnp.int32, (lanes, rows), 0)
+    hits = jnp.zeros((lanes, rows), f32)
+    for k in range(routes_ref.shape[0]):
+        hits = jnp.where(routes_ref[k : k + 1, :] + router_at == lane_row, 1.0, hits)
+    hits_all[me] = hits.T.astype(bf16)
+
+    arrived(w_query)
+    queries = jnp.dot(normed_ref[...], w_query[...], preferred_element_type=f32)
+    queries = queries.astype(bf16).astype(f32)
+    for h in range(local_heads):
+        query_ref[:, h, :] = queries[:, h * head_dim : (h + 1) * head_dim]
+
+    block_len = min(256, cache_len)
+    after_mask = (
+        lax.broadcasted_iota(jnp.int32, (block_len, block_len), 0)
+        > lax.broadcasted_iota(jnp.int32, (block_len, block_len), 1)
+    ).astype(bf16)
+    position = lax.broadcasted_iota(jnp.int32, (lines, block_len), 1)
+    arrived(bias_ref, lengths_ref)
+    head_row = lax.broadcasted_iota(jnp.int32, (local_heads, local_heads), 0)
+    head_col = lax.broadcasted_iota(jnp.int32, (local_heads, local_heads), 1)
+    bias = jnp.sum(jnp.where(head_row == head_col, bias_ref[...], 0.0), axis=1, keepdims=True)
+    line_seq = lax.broadcasted_iota(jnp.int32, (lines, rows), 0) // local_heads
+    seq_lane = lax.broadcasted_iota(jnp.int32, (lines, rows), 1)
+    lengths_row = lengths_ref[...].astype(f32)
+
+    def attend(c, carry):
+        keys_load(c).wait()
+        for i in range(span):
+            s = c * span + i
+            score_ref[s] = (
+                jnp.dot(query_ref[s].astype(bf16), keys[s], preferred_element_type=f32)
+                * head_dim ** (-0.5)
+                + bias
+            )
+        limits = jnp.sum(
+            jnp.where(seq_lane == line_seq + c * span, lengths_row, 0.0), axis=1, keepdims=True
+        ).astype(jnp.int32)
+        later = jnp.zeros((lines, 1), f32)
+        for first_pos in range(cache_len - block_len, -1, -block_len):
+            columns = slice(first_pos, first_pos + block_len)
+            scores = score_ref[pl.ds(c * span, span), :, columns].reshape(lines, block_len)
+            visible = position + first_pos < limits
+            keep = -(jnp.maximum(scores, 0.0) + jnp.log1p(jnp.exp(-jnp.abs(scores))))
+            log_take = scores + keep
+            keep = jnp.where(visible, keep, 0.0)
+            top = keep.astype(bf16)
+            rest = keep - top.astype(f32)
+            middle = rest.astype(bf16)
+            low = (rest - middle.astype(f32)).astype(bf16)
+            sums = jnp.dot(
+                jnp.concatenate([top, middle, low], axis=0),
+                after_mask,
+                preferred_element_type=f32,
+            )
+            after = sums[:lines] + sums[lines : 2 * lines] + sums[2 * lines :] + later
+            later = later + jnp.sum(keep, axis=-1, keepdims=True)
+            stick = jnp.where(visible, jnp.exp(log_take + after), 0.0)
+            score_ref[pl.ds(c * span, span), :, columns] = stick.reshape(
+                span, local_heads, block_len
+            )
+        values_load(c).wait()
+        for i in range(span):
+            s = c * span + i
+            read_ref[s] = lax.dot_general(
+                score_ref[s].astype(bf16),
+                values[s],
+                (((1,), (1,)), ((), ())),
+                preferred_element_type=f32,
+            )
+        return carry
+
+    steps = rows // span
+    lax.fori_loop(0, steps // 2, attend, 0)
+
+    pl.semaphore_wait(barrier, 2 * n - 1)
+    trades = [
+        remote(
+            w_gate_hbm.at[far, :], w_gate.at[:, mine], pair_sems.at[0, 0], pair_sems.at[1, 0], me, peer
+        ),
+        remote(
+            w_up_hbm.at[far, :], w_up.at[:, mine], pair_sems.at[0, 1], pair_sems.at[1, 1], me, peer
+        ),
+        remote(
+            w_down_hbm.at[:, far], w_down.at[mine, :], pair_sems.at[0, 2], pair_sems.at[1, 2], me, peer
+        ),
+    ]
+    for trade in trades:
+        trade.start()
+
+    def small_copy(other, tp):
+        return remote(
+            small_send.at[other],
+            small.at[pl.ds(core * 2 * units, 2 * units), pl.ds(pl.multiple_of(slot * width, width), width)],
+            small_send_sem.at[other],
+            small_recv_sem.at[core, slot],
+            other,
+            tp,
+        )
+
+    def down_copy(other, tp):
+        return remote(
+            down_ref.at[pl.ds(pl.multiple_of(other * units, units), units), :],
+            w_down.at[
+                pl.ds(2 * hidden + core * 2 * units, units),
+                pl.ds(pl.multiple_of(slot * width, width), width),
+            ],
+            down_send_sem.at[other],
+            down_recv_sem.at[core, slot],
+            other,
+            tp,
+        )
+
+    def hits_copy(origin, other):
+        return remote(
+            hits_all.at[origin],
+            hits_all.at[origin],
+            hits_sems.at[0, other],
+            hits_sems.at[1, origin],
+            other,
+            core,
+        )
+
+    arrived(router_ref, mix_ref, down_ref)
+    spread_rows = lanes - mix_at
+    mix_row = mix_ref[...]
+    mix_top = mix_row.astype(bf16)
+    mix_rest = mix_row - mix_top.astype(f32)
+    mix_mid = mix_rest.astype(bf16)
+    mix_low = (mix_rest - mix_mid.astype(f32)).astype(bf16)
+    mix_index = lax.broadcasted_iota(jnp.int32, (spread_rows, model), 0)
+    mix_rows = jnp.where(
+        mix_index == 0,
+        mix_top.astype(f32),
+        jnp.where(
+            mix_index == 1,
+            mix_mid.astype(f32),
+            jnp.where(mix_index == 2, mix_low.astype(f32), 0.0),
+        ),
+    ).astype(bf16)
+    small[pl.ds(router_at, expert_total), :] = jnp.where(
+        core == 0, router_ref[:, :half], router_ref[:, half:]
+    )
+    small[pl.ds(mix_at, spread_rows), :] = jnp.where(
+        core == 0, mix_rows[:, :half], mix_rows[:, half:]
+    )
+    for base in (units, 3 * units):
+        w_down[pl.ds(2 * hidden + base, units), :] = jnp.zeros((units, half), bf16)
+    tail = lanes - 4 * units
+    w_down[pl.ds(2 * hidden + 4 * units, tail), :] = jnp.zeros((tail, half), bf16)
+
+    def send_small(k, carry):
+        other = lax.rem(me + k, n)
+        small_copy(other, owner).start()
+        down_copy(other, owner).start()
+        hits_copy(me, other).start()
+        return carry
+
+    lax.fori_loop(1, n, send_small, 0)
+
+    @pl.when(owner == core)
+    def _():
+        here = pl.ds(pl.multiple_of(slot * width, width), width)
+        small[pl.ds(pl.multiple_of(core * 2 * units, 2 * units), 2 * units), here] = small_send[me]
+        w_down[
+            pl.ds(pl.multiple_of(2 * hidden + core * 2 * units, units), units), here
+        ] = down_ref[pl.ds(pl.multiple_of(me * units, units), units), :]
+
+    @pl.when(owner != core)
+    def _():
+        small_copy(me, peer).start()
+        down_copy(me, peer).start()
+
+    lax.fori_loop(steps // 2, steps, attend, 0)
+    heads_out = jnp.concatenate([read_ref[:, h, :] for h in range(local_heads)], axis=1).astype(
+        bf16
+    )
+    arrived(w_out)
+    swaps = []
+    for i in range(2):
+        attn_mine[i] = jnp.dot(
+            heads_out, w_out[:, i * half : (i + 1) * half], preferred_element_type=f32
+        ).astype(bf16)
+        swaps.append(
+            remote(
+                attn_mine.at[i], attn_peer.at[i], swap_sems.at[0, i], swap_sems.at[1, i], me, peer
+            )
+        )
+        swaps[i].start()
+    arrived(gain_ref)
+    wide = []
+    for i in range(2):
+        swaps[i].wait_recv()
+        columns = slice(i * half, (i + 1) * half)
+        res_ref[i] = (
+            tokens_ref[:, columns].astype(f32)
+            + (attn_mine[i].astype(f32) + attn_peer[i].astype(f32))
+        ).astype(bf16)
+        wide.append(res_ref[i].astype(f32))
+    squares = sum(jnp.sum(part * part, axis=-1, keepdims=True) for part in wide)
+    scale = lax.rsqrt(squares / model + 1e-06)
+    norm_all[me] = (
+        jnp.where(core == 0, wide[0], wide[1])
+        * scale
+        * jnp.where(core == 0, gain_ref[:, :half], gain_ref[:, half:])
+    ).astype(bf16)
+
+    def line_copy(k):
+        return remote(
+            norm_all.at[me],
+            norm_all.at[me],
+            line_sems.at[0, k],
+            line_sems.at[1, k],
+            flip(z, k) * inner + p,
+            core,
+        )
+
+    def spread_copy(k, j):
+        origin = flip(z, k) * inner + p
+        return remote(
+            norm_all.at[origin],
+            norm_all.at[origin],
+            spread_sems.at[0, k, j],
+            spread_sems.at[1, k, j],
+            z * inner + flip(p, j),
+            core,
+        )
+
+    for k in range(1, outer):
+        line_copy(k).start()
+    for j in range(1, inner):
+        spread_copy(0, j).start()
+
+    across = (((1,), (1,)), ((), ()))
+    arrived(w_key_ref, w_value_ref)
+    for weight, target in ((w_key_ref, new_keys_ref), (w_value_ref, new_values_ref)):
+        target[...] = lax.dot_general(
+            normed_ref[...], weight[...], across, preferred_element_type=f32
+        ).astype(bf16)
+
+    def take_small(k, carry):
+        source = core * side + k
+
+        @pl.when(source != me)
+        def _():
+            remote(
+                small_send.at[0],
+                small.at[
+                    pl.ds(core * 2 * units, 2 * units), pl.ds(pl.multiple_of(k * width, width), width)
+                ],
+                small_send_sem.at[0],
+                small_recv_sem.at[core, k],
+                me,
+                peer,
+            ).wait_recv()
+            remote(
+                down_ref.at[pl.ds(0, units), :],
+                w_down.at[
+                    pl.ds(2 * hidden + core * 2 * units, units),
+                    pl.ds(pl.multiple_of(k * width, width), width),
+                ],
+                down_send_sem.at[0],
+                down_recv_sem.at[core, k],
+                me,
+                peer,
+            ).wait_recv()
+
+        remote(
+            small_send.at[0],
+            small.at[
+                pl.ds(peer * 2 * units, 2 * units), pl.ds(pl.multiple_of(k * width, width), width)
+            ],
+            small_send_sem.at[0],
+            small_recv_sem.at[peer, k],
+            me,
+            peer,
+        ).wait_recv()
+        remote(
+            down_ref.at[pl.ds(0, units), :],
+            w_down.at[
+                pl.ds(2 * hidden + peer * 2 * units, units),
+                pl.ds(pl.multiple_of(k * width, width), width),
+            ],
+            down_send_sem.at[0],
+            down_recv_sem.at[peer, k],
+            me,
+            peer,
+        ).wait_recv()
+        return carry
+
+    lax.fori_loop(0, side, take_small, 0)
+
+    def take_hits(k, carry):
+        hits_copy(lax.rem(me + n - k, n), me).wait_recv()
+        return carry
+
+    lax.fori_loop(1, n, take_hits, 0)
+    arrived(*[target for _, target in pairs[15:]])
+    for trade in trades:
+        trade.wait_recv()
+
+    for k in range(1, outer):
+        line_copy(k).wait_recv()
+        for j in range(1, inner):
+            spread_copy(k, j).start()
+
+    chunk = inner * rows
+    lane = lax.broadcasted_iota(jnp.int32, (chunk, lanes), 1)
+    routed = (lane >= router_at) & (lane < mix_at)
+    dense_lane = (lane < units) | ((lane >= 2 * units) & (lane < 3 * units))
+
+    def first_copy(k):
+        return remote(
+            first_send.at[k], first_recv.at[k], first_sems.at[0, k], first_sems.at[1, k], me, peer
+        )
+
+    def group(k):
+        return pl.ds(pl.multiple_of(flip(z, k) * inner, inner), inner)
+
+    def first(k):
+        for j in range(1, inner):
+            spread_copy(k, j).wait_recv()
+        x = norm_all[group(k)].reshape(chunk, half)
+        first_send[k, :, : 2 * hidden] = jnp.dot(x, w_gate[...], preferred_element_type=f32)
+        first_send[k, :, 2 * hidden : 4 * hidden] = jnp.dot(
+            x, w_up[...], preferred_element_type=f32
+        )
+        first_send[k, :, 4 * hidden :] = lax.dot_general(
+            x, small[...], across, preferred_element_type=f32
+        )
+        first_copy(k).start()
+
+    def plane_copy(k, j):
+        other = flip(p, j)
+        return remote(
+            plane_send.at[k, other],
+            plane_recv.at[k, j],
+            plane_sems.at[0, k, j],
+            plane_sems.at[1, k, j],
+            z * inner + other,
+            core,
+        )
+
+    def second(k):
+        first_copy(k).wait_recv()
+        gate_rows = first_send[k, :, : 2 * hidden] + first_recv[k, :, : 2 * hidden]
+        up_rows = (
+            first_send[k, :, 2 * hidden : 4 * hidden] + first_recv[k, :, 2 * hidden : 4 * hidden]
+        )
+        rest = first_send[k, :, 4 * hidden :] + first_recv[k, :, 4 * hidden :]
+        chosen = hits_all[group(k)].reshape(chunk, lanes).astype(f32)
+        picked = jnp.where(routed & (chosen > 0.0), jax.nn.sigmoid(rest), 0.0)
+        total = jnp.sum(picked, axis=-1, keepdims=True)
+        own = jnp.sum(jnp.where(lane == router_at + me, picked, 0.0), axis=-1, keepdims=True)
+        gate = own / total * 2.5
+        mix_sum = jnp.sum(jnp.where(lane >= mix_at, rest, 0.0), axis=-1, keepdims=True)
+        mix_gate = jax.nn.sigmoid(mix_sum)
+        dense = jax.nn.silu(rest) * pltpu.roll(rest, lanes - units, 1) * mix_gate
+        dense = jnp.where(dense_lane, dense, 0.0).astype(bf16)
+        act = (jax.nn.silu(gate_rows) * up_rows * gate).astype(bf16)
+        value = jnp.dot(act, w_down[: 2 * hidden], preferred_element_type=f32) + jnp.dot(
+            dense, w_down[2 * hidden :], preferred_element_type=f32
+        )
+        plane_send[k] = value.astype(bf16).reshape(inner, rows, half)
+        for j in range(inner - 1, 0, -1):
+            plane_copy(k, j).start()
+
+    def back_copy(k):
+        return remote(
+            line_send.at[k],
+            line_recv.at[k],
+            back_sems.at[0, k],
+            back_sems.at[1, k],
+            flip(z, k) * inner + p,
+            core,
+        )
+
+    def collect(k):
+        total = plane_send[k, p].astype(f32)
+        for j in range(1, inner):
+            plane_copy(k, j).wait_recv()
+            total = total + plane_recv[k, j].astype(f32)
+        return total
+
+    def third(k):
+        line_send[k] = collect(k).astype(bf16)
+        back_copy(k).start()
+
+    first(0)
+    for k in range(1, outer):
+        first(k)
+        second(k - 1)
+    second(outer - 1)
+    for k in range(1, outer):
+        third(k)
+    total = res_ref[core].astype(f32) + collect(0)
+    for k in range(1, outer):
+        back_copy(k).wait_recv()
+        total = total + line_recv[k].astype(f32)
+    out_ref[...] = total.astype(bf16)
+
+    def drain(k, carry):
+        other = lax.rem(me + k, n)
+        small_copy(other, owner).wait_send()
+        down_copy(other, owner).wait_send()
+        hits_copy(me, other).wait_send()
+        return carry
+
+    lax.fori_loop(1, n, drain, 0)
+
+    @pl.when(owner != core)
+    def _():
+        small_copy(me, peer).wait_send()
+        down_copy(me, peer).wait_send()
+
+    for copy in trades + swaps:
+        copy.wait_send()
+    for k in range(outer):
+        if k:
+            line_copy(k).wait_send()
+            back_copy(k).wait_send()
+        first_copy(k).wait_send()
+        for j in range(1, inner):
+            spread_copy(k, j).wait_send()
+            plane_copy(k, j).wait_send()
+
+
+def routed_shards(n, inner, arrays):
+    tokens = arrays[0]
+    w_key, head_bias = arrays[4], arrays[3]
+    keys, w_gate, w_down = arrays[18], arrays[15], arrays[17]
+    rows, model = tokens.shape
+    half = model // 2
+    width, hidden_cols = arrays[10].shape
+    units = hidden_cols // n
+    outer = n // inner
+    seq_count, head_dim, cache_len = keys.shape
+    local_heads = head_bias.shape[1]
+    hidden = w_gate.shape[1]
+    lanes = 128
+    chunk = inner * rows
+    bf16, f32 = jnp.bfloat16, jnp.float32
+    vmem = pl.BlockSpec(memory_space=pltpu.VMEM)
+    anywhere = pl.BlockSpec(memory_space=pltpu.HBM)
+    dma = pltpu.SemaphoreType.DMA
+    small_inputs = [pltpu.VMEM(a.shape, a.dtype) for a in arrays[:15]]
+    return pl.pallas_call(
+        functools.partial(routed_layer, n, inner),
+        out_shape=(
+            jax.ShapeDtypeStruct((rows, half), bf16),
+            jax.ShapeDtypeStruct((rows, w_key.shape[0]), bf16),
+            jax.ShapeDtypeStruct((rows, w_key.shape[0]), bf16),
+        ),
+        in_specs=[anywhere] * 20,
+        out_specs=(vmem, vmem, vmem),
+        scratch_shapes=small_inputs
+        + [
+            pltpu.VMEM((half, 2 * hidden), bf16),
+            pltpu.VMEM((half, 2 * hidden), bf16),
+            pltpu.VMEM((2 * hidden + lanes, half), bf16),
+            pltpu.VMEM(keys.shape, bf16),
+            pltpu.VMEM(keys.shape, bf16),
+            pltpu.VMEM((rows, local_heads, head_dim), f32),
+            pltpu.VMEM((rows, local_heads, cache_len), f32),
+            pltpu.VMEM((rows, local_heads, head_dim), f32),
+            pltpu.VMEM((rows, model), bf16),
+            pltpu.VMEM((n, 2 * units, width), bf16),
+            pltpu.VMEM((lanes, half), bf16),
+            pltpu.VMEM((n, rows, lanes), bf16),
+            pltpu.VMEM((2, rows, half), bf16),
+            pltpu.VMEM((2, rows, half), bf16),
+            pltpu.VMEM((2, rows, half), bf16),
+            pltpu.VMEM((n, rows, half), bf16),
+            pltpu.VMEM((outer, chunk, 4 * hidden + lanes), f32),
+            pltpu.VMEM((outer, chunk, 4 * hidden + lanes), f32),
+            pltpu.VMEM((outer, inner, rows, half), bf16),
+            pltpu.VMEM((outer, inner, rows, half), bf16),
+            pltpu.VMEM((outer, rows, half), bf16),
+            pltpu.VMEM((outer, rows, half), bf16),
+            dma((18,)),
+            dma((rows // 4,)),
+            dma((rows // 4,)),
+            dma((2, 3)),
+            dma((2, 2)),
+            dma((n,)),
+            dma((2, n // 2)),
+            dma((n,)),
+            dma((2, n // 2)),
+            dma((2, n)),
+            dma((2, outer)),
+            dma((2, outer, inner)),
+            dma((2, outer)),
+            dma((2, outer, inner)),
+            dma((2, outer)),
+        ],
+        compiler_params=pltpu.CompilerParams(
+            collective_id=0, has_side_effects=True, vmem_limit_bytes=48 * 1024 * 1024
+        ),
+        name="routed_layer",
+    )(*[pltpu.with_memory_space_constraint(a, pltpu.HBM) for a in arrays])
+
+
 def shards(
     n,
     tokens,
@@ -597,6 +1289,34 @@
     values = value_cache.reshape(seq_count, head_dim, cache_len)
     w_gate, w_up, w_down = w_expert_gate[0], w_expert_up[0], w_expert_down[0]
     expert_hidden = w_gate.shape[1]
+    arrays = (
+        tokens,
+        attn_gain.reshape(1, model),
+        lengths.reshape(1, seq_count),
+        head_bias.reshape(1, local_heads),
+        w_key.T,
+        w_value.T,
+        ffn_gain.reshape(1, model),
+        w_router.T,
+        routes.T,
+        dense_mix.reshape(1, model),
+        w_dense_gate,
+        w_dense_up,
+        w_dense_down,
+        w_query,
+        w_attn_out,
+        w_gate,
+        w_up,
+        w_down,
+        keys,
+        values,
+    )
+    inner = 1
+    while (2 * inner) ** 2 <= n:
+        inner *= 2
+    small_rows = 4 * (hidden_cols // n) + w_router.shape[1]
+    if hidden_cols % (16 * n) == 0 and width % 128 == 0 and small_rows <= 112:
+        return routed_shards(n, inner, arrays)
     bf16, f32 = jnp.bfloat16, jnp.float32
     block = min(n, 16) * rows
     vmem = pl.BlockSpec(memory_space=pltpu.VMEM)
@@ -660,28 +1380,7 @@
             collective_id=0, has_side_effects=True, vmem_limit_bytes=63 * 1024 * 1024
         ),
         name="whole_layer",
-    )(
-        tokens,
-        attn_gain.reshape(1, model),
-        lengths.reshape(1, seq_count),
-        head_bias.reshape(1, local_heads),
-        w_key.T,
-        w_value.T,
-        ffn_gain.reshape(1, model),
-        w_router.T,
-        routes.T,
-        dense_mix.reshape(1, model),
-        w_dense_gate,
-        w_dense_up,
-        w_dense_down,
-        w_query,
-        w_attn_out,
-        w_gate,
-        w_up,
-        w_down,
-        keys,
-        values,
-    )
+    )(*arrays)
 
 
 def solution(mesh):

time: 54.6 us -> 38.6 us (0.71)
  the two profiles are of different devices: /device:TPU:7 before, /device:TPU:0 now
where the time goes in v1:
time: 38.6 us; the launch traced here: 38.4 us
  Pallas kernels  36 us (93%)
  local copies, waits for them, and re-layouts  1.8 us (5%)
  between operations  0.65 us (2%)
    pallas_call x1, Pallas kernels, routed_shards(): pl.pallas_call(functools.partial(routed_layer, n, inner), out_shape=(jax....  36 us
    unnamed x3, local copies, waits for them, and re-layouts  1.8 us

profile of v1, /device:TPU:0, one launch (start us, length us, event | category | flops | bytes accessed | tf_op | source)
XLA Modules:
  0.0 38.4 jit_solution(16442759193982687439)
XLA Ops:
  0.6 36.0 %routed_layer.1 = (bf16[16,1024]{1,0:T(8,128)(2,1)S(1)}, bf16[16,64]{1,0:T(8,128)(2,1)S(1)}, bf16[16,64]{1,0:T(8,128)(2,1)S(1)}) custom-call(bf16[16,2048]{1,0:T(8,128)(2,1)} %tokens_hbm.1, f32[1,2048]{1,0:T(1,128)} %bitcast.22, s32[1,16]{1,0:T(1,128)} %bitcast.26, f32[1,8]{1,0:T(1,128)} %bitcast.27, bf16[64,2048]{1,0:T(8,128)(2,1)} %bitcast.19, ...), custom_call_target="tpu_custom_call" | custom-call | tf_op jit(solution)/shard_map/routed_layer/pallas_call | solution.py:1201
  36.6 0.6 %copy.26 = bf16[16,1024]{1,0:T(8,128)(2,1)} copy(bf16[16,1024]{1,0:T(8,128)(2,1)S(1)} %get-tuple-element.6) | data formatting | bytes 65536
  37.2 0.6 %copy.27 = bf16[16,64]{1,0:T(8,128)(2,1)} copy(bf16[16,64]{1,0:T(8,128)(2,1)S(1)} %get-tuple-element.7) | data formatting | bytes 4096
  37.8 0.6 %copy.28 = bf16[16,64]{1,0:T(8,128)(2,1)} copy(bf16[16,64]{1,0:T(8,128)(2,1)S(1)} %get-tuple-element.8) | data formatting | bytes 4096

commit v2 on v1

--- a/solution.py
+++ b/solution.py
@@ -571,6 +571,16 @@
     return result
 
 
+def finish(*refs):
+    copies = [
+        pltpu.make_async_copy(refs[i], refs[i + 3], refs[6].at[i]) for i in range(3)
+    ]
+    for copy in copies:
+        copy.start()
+    for copy in copies:
+        copy.wait()
+
+
 def routed_layer(
     n,
     inner,
@@ -620,10 +630,12 @@
     query_ref,
     score_ref,
     read_ref,
+    stick_ref,
     normed_ref,
     small_send,
     small,
-    hits_all,
+    routes_all,
+    hits_ref,
     attn_mine,
     attn_peer,
     res_ref,
@@ -632,6 +644,7 @@
     first_recv,
     plane_send,
     plane_recv,
+    far_recv,
     line_send,
     line_recv,
     load_sem,
@@ -643,11 +656,12 @@
     small_recv_sem,
     down_send_sem,
     down_recv_sem,
-    hits_sems,
+    routes_sems,
     line_sems,
     spread_sems,
     first_sems,
     plane_sems,
+    far_sems,
     back_sems,
 ):
     me = lax.axis_index("ep")
@@ -669,7 +683,10 @@
     lanes = small.shape[0]
     router_at = 4 * units
     mix_at = router_at + expert_total
-    span = 4
+    span = rows // 2
+    turns = list(range(outer - 1, 0, -1))
+    direct = [j for j in range(1, inner) if j & (j - 1) == 0]
+    indirect = [j for j in range(1, inner) if j & (j - 1)]
     lines = span * local_heads
 
     def remote(source, target, send_sem, recv_sem, ep, tp):
@@ -685,18 +702,20 @@
     near = pl.ds(pl.multiple_of(core * half, half), half)
     far = pl.ds(pl.multiple_of(peer * half, half), half)
     mine = pl.ds(pl.multiple_of(core * hidden, hidden), hidden)
+    quarter = model // 4
+    query_parts = [pl.ds(i * quarter, quarter) for i in range(4)]
     pairs = (
         (tokens_hbm, tokens_ref),
         (attn_gain_hbm, attn_gain_ref),
         (dense_gate_hbm, dense_gate_ref),
         (dense_up_hbm, dense_up_ref),
         (routes_hbm, routes_ref),
-        (w_query_hbm, w_query),
+        *[(w_query_hbm.at[part], w_query.at[part]) for part in query_parts],
         (bias_hbm, bias_ref),
         (lengths_hbm, lengths_ref),
+        (down_hbm, down_ref),
         (router_hbm, router_ref),
         (mix_hbm, mix_ref),
-        (down_hbm, down_ref),
         (gain_hbm, gain_ref),
         (w_out_hbm, w_out),
         (w_key_hbm, w_key_ref),
@@ -723,12 +742,7 @@
         block = pl.ds(c * span, span)
         return pltpu.make_async_copy(values_hbm.at[block], values.at[block], values_sem.at[c])
 
-    for load in loads[:8]:
-        load.start()
-    for c in range(rows // span):
-        keys_load(c).start()
-        values_load(c).start()
-    for load in loads[8:]:
+    for load in loads[:12]:
         load.start()
 
     barrier = pltpu.get_barrier_semaphore()
@@ -749,17 +763,24 @@
         * lax.rsqrt(jnp.mean(start * start, axis=-1, keepdims=True) + 1e-06)
         * attn_gain_ref[...]
     ).astype(bf16)
+    for c in range(2):
+        keys_load(c).start()
     arrived(dense_gate_ref, dense_up_ref, routes_ref)
     small_send[:, :units, :] = dense_gate_ref[...].T.reshape(n, units, width)
     small_send[:, units:, :] = dense_up_ref[...].T.reshape(n, units, width)
-    lane_row = lax.broadcasted_iota(jnp.int32, (lanes, rows), 0)
-    hits = jnp.zeros((lanes, rows), f32)
-    for k in range(routes_ref.shape[0]):
-        hits = jnp.where(routes_ref[k : k + 1, :] + router_at == lane_row, 1.0, hits)
-    hits_all[me] = hits.T.astype(bf16)
-
-    arrived(w_query)
-    queries = jnp.dot(normed_ref[...], w_query[...], preferred_element_type=f32)
+    top_k = routes_ref.shape[0]
+    for k in range(top_k):
+        routes_all[me, :, k * rows : (k + 1) * rows] = routes_ref[k : k + 1, :].astype(f32)
+
+    queries = jnp.zeros((rows, w_query.shape[1]), f32)
+    for i in range(4):
+        loads[5 + i].wait()
+        if i % 2:
+            values_load(i // 2).start()
+        part = slice(i * quarter, (i + 1) * quarter)
+        queries = queries + jnp.dot(
+            normed_ref[:, part], w_query[part, :], preferred_element_type=f32
+        )
     queries = queries.astype(bf16).astype(f32)
     for h in range(local_heads):
         query_ref[:, h, :] = queries[:, h * head_dim : (h + 1) * head_dim]
@@ -778,54 +799,51 @@
     seq_lane = lax.broadcasted_iota(jnp.int32, (lines, rows), 1)
     lengths_row = lengths_ref[...].astype(f32)
 
-    def attend(c, carry):
-        keys_load(c).wait()
-        for i in range(span):
-            s = c * span + i
-            score_ref[s] = (
-                jnp.dot(query_ref[s].astype(bf16), keys[s], preferred_element_type=f32)
-                * head_dim ** (-0.5)
-                + bias
-            )
+    for s in range(rows):
+        if s % span == 0:
+            keys_load(s // span).wait()
+            for load in loads[12:16] if s == 0 else loads[16:]:
+                load.start()
+        score_ref[s] = (
+            jnp.dot(query_ref[s].astype(bf16), keys[s], preferred_element_type=f32)
+            * head_dim ** (-0.5)
+            + bias
+        )
+
+    def stick_breaking(c):
         limits = jnp.sum(
             jnp.where(seq_lane == line_seq + c * span, lengths_row, 0.0), axis=1, keepdims=True
         ).astype(jnp.int32)
         later = jnp.zeros((lines, 1), f32)
         for first_pos in range(cache_len - block_len, -1, -block_len):
             columns = slice(first_pos, first_pos + block_len)
-            scores = score_ref[pl.ds(c * span, span), :, columns].reshape(lines, block_len)
+            scores = score_ref[c * span : (c + 1) * span, :, columns].reshape(lines, block_len)
             visible = position + first_pos < limits
-            keep = -(jnp.maximum(scores, 0.0) + jnp.log1p(jnp.exp(-jnp.abs(scores))))
+            keep = -(jnp.maximum(scores, 0.0) + jnp.log(1.0 + jnp.exp(-jnp.abs(scores))))
             log_take = scores + keep
             keep = jnp.where(visible, keep, 0.0)
             top = keep.astype(bf16)
-            rest = keep - top.astype(f32)
-            middle = rest.astype(bf16)
-            low = (rest - middle.astype(f32)).astype(bf16)
+            low = (keep - top.astype(f32)).astype(bf16)
             sums = jnp.dot(
-                jnp.concatenate([top, middle, low], axis=0),
-                after_mask,
-                preferred_element_type=f32,
+                jnp.concatenate([top, low], axis=0), after_mask, preferred_element_type=f32
             )
-            after = sums[:lines] + sums[lines : 2 * lines] + sums[2 * lines :] + later
+            after = sums[:lines] + sums[lines:] + later
             later = later + jnp.sum(keep, axis=-1, keepdims=True)
             stick = jnp.where(visible, jnp.exp(log_take + after), 0.0)
-            score_ref[pl.ds(c * span, span), :, columns] = stick.reshape(
-                span, local_heads, block_len
-            )
-        values_load(c).wait()
-        for i in range(span):
-            s = c * span + i
-            read_ref[s] = lax.dot_general(
-                score_ref[s].astype(bf16),
-                values[s],
-                (((1,), (1,)), ((), ())),
-                preferred_element_type=f32,
-            )
-        return carry
-
-    steps = rows // span
-    lax.fori_loop(0, steps // 2, attend, 0)
+            stick_ref[c, :, columns] = stick.astype(bf16)
+
+    def read_values(c):
+        mixed = lax.dot_general(
+            values[c * span : (c + 1) * span].reshape(span * head_dim, cache_len),
+            stick_ref[c],
+            (((1,), (1,)), ((), ())),
+            preferred_element_type=f32,
+        ).reshape(span, head_dim, lines)
+        seq_of = lax.broadcasted_iota(jnp.int32, (head_dim, lines), 1) // local_heads
+        own_seq = jnp.zeros((head_dim, lines), f32)
+        for s in range(span):
+            own_seq = jnp.where(seq_of == s, mixed[s], own_seq)
+        read_ref[c * span : (c + 1) * span] = own_seq.T.reshape(span, local_heads, head_dim)
 
     pl.semaphore_wait(barrier, 2 * n - 1)
     trades = [
@@ -839,8 +857,6 @@
             w_down_hbm.at[:, far], w_down.at[mine, :], pair_sems.at[0, 2], pair_sems.at[1, 2], me, peer
         ),
     ]
-    for trade in trades:
-        trade.start()
 
     def small_copy(other, tp):
         return remote(
@@ -865,17 +881,159 @@
             tp,
         )
 
-    def hits_copy(origin, other):
-        return remote(
-            hits_all.at[origin],
-            hits_all.at[origin],
-            hits_sems.at[0, other],
-            hits_sems.at[1, origin],
+    def routes_copy(origin, other):
+        return remote(
+            routes_all.at[origin],
+            routes_all.at[origin],
+            routes_sems.at[0, other],
+            routes_sems.at[1, origin],
             other,
             core,
         )
 
-    arrived(router_ref, mix_ref, down_ref)
+    arrived(down_ref)
+
+    def send_small(k, carry):
+        other = lax.rem(me + k, n)
+        routes_copy(me, other).start()
+        small_copy(other, owner).start()
+        return carry
+
+    def send_down(k, carry):
+        down_copy(lax.rem(me + k, n), owner).start()
+        return carry
+
+    lax.fori_loop(1, n, send_small, 0)
+
+    @pl.when(owner == core)
+    def _():
+        here = pl.ds(pl.multiple_of(slot * width, width), width)
+        small[pl.ds(pl.multiple_of(core * 2 * units, 2 * units), 2 * units), here] = small_send[me]
+        w_down[
+            pl.ds(pl.multiple_of(2 * hidden + core * 2 * units, units), units), here
+        ] = down_ref[pl.ds(pl.multiple_of(me * units, units), units), :]
+
+    @pl.when(owner != core)
+    def _():
+        small_copy(me, peer).start()
+
+    for c in range(2):
+        values_load(c).wait()
+    for c in range(2):
+        stick_breaking(c)
+        read_values(c)
+    heads_out = jnp.concatenate([read_ref[:, h, :] for h in range(local_heads)], axis=1).astype(
+        bf16
+    )
+    arrived(w_out)
+    swaps = []
+    for i in range(2):
+        attn_mine[i] = jnp.dot(
+            heads_out, w_out[:, i * half : (i + 1) * half], preferred_element_type=f32
+        ).astype(bf16)
+        swaps.append(
+            remote(
+                attn_mine.at[i], attn_peer.at[i], swap_sems.at[0, i], swap_sems.at[1, i], me, peer
+            )
+        )
+        swaps[i].start()
+    for trade in trades:
+        trade.start()
+    arrived(gain_ref)
+    wide = []
+    for i in range(2):
+        swaps[i].wait_recv()
+        columns = slice(i * half, (i + 1) * half)
+        res_ref[i] = (
+            tokens_ref[:, columns].astype(f32)
+            + (attn_mine[i].astype(f32) + attn_peer[i].astype(f32))
+        ).astype(bf16)
+        wide.append(res_ref[i].astype(f32))
+    squares = sum(jnp.sum(part * part, axis=-1, keepdims=True) for part in wide)
+    scale = lax.rsqrt(squares / model + 1e-06)
+    norm_all[me] = (
+        jnp.where(core == 0, wide[0], wide[1])
+        * scale
+        * jnp.where(core == 0, gain_ref[:, :half], gain_ref[:, half:])
+    ).astype(bf16)
+
+    def line_copy(k):
+        return remote(
+            norm_all.at[me],
+            norm_all.at[me],
+            line_sems.at[0, k],
+            line_sems.at[1, k],
+            flip(z, k) * inner + p,
+            core,
+        )
+
+    def spread_copy(k, j):
+        origin = flip(z, k) * inner + p
+        return remote(
+            norm_all.at[origin],
+            norm_all.at[origin],
+            spread_sems.at[0, k, j],
+            spread_sems.at[1, k, j],
+            z * inner + flip(p, j),
+            core,
+        )
+
+    for k in turns:
+        line_copy(k).start()
+    for j in indirect + direct:
+        spread_copy(0, j).start()
+
+    lax.fori_loop(1, n, send_down, 0)
+
+    @pl.when(owner != core)
+    def _():
+        down_copy(me, peer).start()
+
+
+    across = (((1,), (1,)), ((), ()))
+    arrived(w_key_ref, w_value_ref)
+    for weight, target in ((w_key_ref, new_keys_ref), (w_value_ref, new_values_ref)):
+        target[...] = lax.dot_general(
+            normed_ref[...], weight[...], across, preferred_element_type=f32
+        ).astype(bf16)
+
+    def small_taken(tp, k):
+        return remote(
+            small_send.at[0],
+            small.at[
+                pl.ds(tp * 2 * units, 2 * units), pl.ds(pl.multiple_of(k * width, width), width)
+            ],
+            small_send_sem.at[0],
+            small_recv_sem.at[tp, k],
+            me,
+            peer,
+        )
+
+    def down_taken(tp, k):
+        return remote(
+            down_ref.at[pl.ds(0, units), :],
+            w_down.at[
+                pl.ds(2 * hidden + tp * 2 * units, units),
+                pl.ds(pl.multiple_of(k * width, width), width),
+            ],
+            down_send_sem.at[0],
+            down_recv_sem.at[tp, k],
+            me,
+            peer,
+        )
+
+    def take_all(taken):
+        def take(k, carry):
+            @pl.when(core * side + k != me)
+            def _():
+                taken(core, k).wait_recv()
+
+            taken(peer, k).wait_recv()
+            return carry
+
+        lax.fori_loop(0, side, take, 0)
+
+    arrived(router_ref, mix_ref)
     spread_rows = lanes - mix_at
     mix_row = mix_ref[...]
     mix_top = mix_row.astype(bf16)
@@ -903,165 +1061,21 @@
     tail = lanes - 4 * units
     w_down[pl.ds(2 * hidden + 4 * units, tail), :] = jnp.zeros((tail, half), bf16)
 
-    def send_small(k, carry):
-        other = lax.rem(me + k, n)
-        small_copy(other, owner).start()
-        down_copy(other, owner).start()
-        hits_copy(me, other).start()
-        return carry
-
-    lax.fori_loop(1, n, send_small, 0)
-
-    @pl.when(owner == core)
-    def _():
-        here = pl.ds(pl.multiple_of(slot * width, width), width)
-        small[pl.ds(pl.multiple_of(core * 2 * units, 2 * units), 2 * units), here] = small_send[me]
-        w_down[
-            pl.ds(pl.multiple_of(2 * hidden + core * 2 * units, units), units), here
-        ] = down_ref[pl.ds(pl.multiple_of(me * units, units), units), :]
-
-    @pl.when(owner != core)
-    def _():
-        small_copy(me, peer).start()
-        down_copy(me, peer).start()
-
-    lax.fori_loop(steps // 2, steps, attend, 0)
-    heads_out = jnp.concatenate([read_ref[:, h, :] for h in range(local_heads)], axis=1).astype(
-        bf16
-    )
-    arrived(w_out)
-    swaps = []
-    for i in range(2):
-        attn_mine[i] = jnp.dot(
-            heads_out, w_out[:, i * half : (i + 1) * half], preferred_element_type=f32
-        ).astype(bf16)
-        swaps.append(
-            remote(
-                attn_mine.at[i], attn_peer.at[i], swap_sems.at[0, i], swap_sems.at[1, i], me, peer
-            )
-        )
-        swaps[i].start()
-    arrived(gain_ref)
-    wide = []
-    for i in range(2):
-        swaps[i].wait_recv()
-        columns = slice(i * half, (i + 1) * half)
-        res_ref[i] = (
-            tokens_ref[:, columns].astype(f32)
-            + (attn_mine[i].astype(f32) + attn_peer[i].astype(f32))
-        ).astype(bf16)
-        wide.append(res_ref[i].astype(f32))
-    squares = sum(jnp.sum(part * part, axis=-1, keepdims=True) for part in wide)
-    scale = lax.rsqrt(squares / model + 1e-06)
-    norm_all[me] = (
-        jnp.where(core == 0, wide[0], wide[1])
-        * scale
-        * jnp.where(core == 0, gain_ref[:, :half], gain_ref[:, half:])
-    ).astype(bf16)
-
-    def line_copy(k):
-        return remote(
-            norm_all.at[me],
-            norm_all.at[me],
-            line_sems.at[0, k],
-            line_sems.at[1, k],
-            flip(z, k) * inner + p,
-            core,
-        )
-
-    def spread_copy(k, j):
-        origin = flip(z, k) * inner + p
-        return remote(
-            norm_all.at[origin],
-            norm_all.at[origin],
-            spread_sems.at[0, k, j],
-            spread_sems.at[1, k, j],
-            z * inner + flip(p, j),
-            core,
-        )
-
-    for k in range(1, outer):
-        line_copy(k).start()
-    for j in range(1, inner):
-        spread_copy(0, j).start()
-
-    across = (((1,), (1,)), ((), ()))
-    arrived(w_key_ref, w_value_ref)
-    for weight, target in ((w_key_ref, new_keys_ref), (w_value_ref, new_values_ref)):
-        target[...] = lax.dot_general(
-            normed_ref[...], weight[...], across, preferred_element_type=f32
-        ).astype(bf16)
-
-    def take_small(k, carry):
-        source = core * side + k
-
-        @pl.when(source != me)
-        def _():
-            remote(
-                small_send.at[0],
-                small.at[
-                    pl.ds(core * 2 * units, 2 * units), pl.ds(pl.multiple_of(k * width, width), width)
-                ],
-                small_send_sem.at[0],
-                small_recv_sem.at[core, k],
-                me,
-                peer,
-            ).wait_recv()
-            remote(
-                down_ref.at[pl.ds(0, units), :],
-                w_down.at[
-                    pl.ds(2 * hidden + core * 2 * units, units),
-                    pl.ds(pl.multiple_of(k * width, width), width),
-                ],
-                down_send_sem.at[0],
-                down_recv_sem.at[core, k],
-                me,
-                peer,
-            ).wait_recv()
-
-        remote(
-            small_send.at[0],
-            small.at[
-                pl.ds(peer * 2 * units, 2 * units), pl.ds(pl.multiple_of(k * width, width), width)
-            ],
-            small_send_sem.at[0],
-            small_recv_sem.at[peer, k],
-            me,
-            peer,
-        ).wait_recv()
-        remote(
-            down_ref.at[pl.ds(0, units), :],
-            w_down.at[
-                pl.ds(2 * hidden + peer * 2 * units, units),
-                pl.ds(pl.multiple_of(k * width, width), width),
-            ],
-            down_send_sem.at[0],
-            down_recv_sem.at[peer, k],
-            me,
-            peer,
-        ).wait_recv()
-        return carry
-
-    lax.fori_loop(0, side, take_small, 0)
-
-    def take_hits(k, carry):
-        hits_copy(lax.rem(me + n - k, n), me).wait_recv()
-        return carry
-
-    lax.fori_loop(1, n, take_hits, 0)
-    arrived(*[target for _, target in pairs[15:]])
+    for k in turns:
+        line_copy(k).wait_recv()
+        for j in indirect + direct:
+            spread_copy(k, j).start()
+    take_all(small_taken)
+
+    arrived(*[target for _, target in pairs[18:]])
     for trade in trades:
         trade.wait_recv()
 
-    for k in range(1, outer):
-        line_copy(k).wait_recv()
-        for j in range(1, inner):
-            spread_copy(k, j).start()
-
     chunk = inner * rows
     lane = lax.broadcasted_iota(jnp.int32, (chunk, lanes), 1)
-    routed = (lane >= router_at) & (lane < mix_at)
     dense_lane = (lane < units) | ((lane >= 2 * units) & (lane < 3 * units))
+
+    rest_at = 2 * hidden + lanes
 
     def first_copy(k):
         return remote(
@@ -1076,12 +1090,10 @@
             spread_copy(k, j).wait_recv()
         x = norm_all[group(k)].reshape(chunk, half)
         first_send[k, :, : 2 * hidden] = jnp.dot(x, w_gate[...], preferred_element_type=f32)
-        first_send[k, :, 2 * hidden : 4 * hidden] = jnp.dot(
-            x, w_up[...], preferred_element_type=f32
-        )
-        first_send[k, :, 4 * hidden :] = lax.dot_general(
+        first_send[k, :, 2 * hidden : rest_at] = lax.dot_general(
             x, small[...], across, preferred_element_type=f32
         )
+        first_send[k, :, rest_at:] = jnp.dot(x, w_up[...], preferred_element_type=f32)
         first_copy(k).start()
 
     def plane_copy(k, j):
@@ -1095,15 +1107,30 @@
             core,
         )
 
+    def far_copy(k, j):
+        return remote(
+            plane_send.at[k, flip(p, j)],
+            far_recv.at[k, j],
+            far_sems.at[0, k, j],
+            far_sems.at[1, k, j],
+            flip(z, k) * inner + p,
+            core,
+        )
+
+    def send_plane(k):
+        for j in direct:
+            plane_copy(k, j).start()
+        if k:
+            for j in indirect:
+                far_copy(k, j).start()
+
     def second(k):
         first_copy(k).wait_recv()
         gate_rows = first_send[k, :, : 2 * hidden] + first_recv[k, :, : 2 * hidden]
-        up_rows = (
-            first_send[k, :, 2 * hidden : 4 * hidden] + first_recv[k, :, 2 * hidden : 4 * hidden]
-        )
-        rest = first_send[k, :, 4 * hidden :] + first_recv[k, :, 4 * hidden :]
-        chosen = hits_all[group(k)].reshape(chunk, lanes).astype(f32)
-        picked = jnp.where(routed & (chosen > 0.0), jax.nn.sigmoid(rest), 0.0)
+        up_rows = first_send[k, :, rest_at:] + first_recv[k, :, rest_at:]
+        rest = first_send[k, :, 2 * hidden : rest_at] + first_recv[k, :, 2 * hidden : rest_at]
+        chosen = hits_ref[group(k)].reshape(chunk, lanes)
+        picked = jnp.where(chosen > 0.0, jax.nn.sigmoid(rest), 0.0)
         total = jnp.sum(picked, axis=-1, keepdims=True)
         own = jnp.sum(jnp.where(lane == router_at + me, picked, 0.0), axis=-1, keepdims=True)
         gate = own / total * 2.5
@@ -1116,8 +1143,17 @@
             dense, w_down[2 * hidden :], preferred_element_type=f32
         )
         plane_send[k] = value.astype(bf16).reshape(inner, rows, half)
-        for j in range(inner - 1, 0, -1):
-            plane_copy(k, j).start()
+        send_plane(k)
+
+    def far_home(j):
+        return remote(
+            far_recv.at[0, j],
+            plane_recv.at[0, j],
+            plane_sems.at[0, 0, j],
+            plane_sems.at[1, 0, j],
+            z * inner + flip(p, j),
+            core,
+        )
 
     def back_copy(k):
         return remote(
@@ -1131,7 +1167,7 @@
 
     def collect(k):
         total = plane_send[k, p].astype(f32)
-        for j in range(1, inner):
+        for j in direct:
             plane_copy(k, j).wait_recv()
             total = total + plane_recv[k, j].astype(f32)
         return total
@@ -1141,23 +1177,50 @@
         back_copy(k).start()
 
     first(0)
-    for k in range(1, outer):
+    def take_routes(k, carry):
+        routes_copy(lax.rem(me + n - k, n), me).wait_recv()
+        return carry
+
+    lax.fori_loop(1, n, take_routes, 0)
+    row_lane = (lax.broadcasted_iota(jnp.int32, (rows, lanes), 1) - router_at).astype(f32)
+    named = routes_all[...].reshape(n, lanes).T
+    for j in range(n):
+        hit = jnp.zeros((rows, lanes), f32)
+        for c in range(top_k):
+            hit = jnp.where(named[c * rows : (c + 1) * rows, j : j + 1] == row_lane, 1.0, hit)
+        hits_ref[j] = hit
+
+    first(turns[0])
+    take_all(down_taken)
+    second(0)
+    for before, k in zip(turns, turns[1:]):
         first(k)
-        second(k - 1)
-    second(outer - 1)
-    for k in range(1, outer):
+        second(before)
+    second(turns[-1])
+    for k in turns:
         third(k)
+    for j in indirect:
+        other = flip(p, j)
+        total = plane_send[0, other].astype(f32)
+        for k in turns:
+            far_copy(k, j).wait_recv()
+            total = total + far_recv[k, j].astype(f32)
+        far_recv[0, j] = total.astype(bf16)
+        far_home(j).start()
     total = res_ref[core].astype(f32) + collect(0)
-    for k in range(1, outer):
+    for k in turns:
         back_copy(k).wait_recv()
         total = total + line_recv[k].astype(f32)
+    for j in indirect:
+        far_home(j).wait_recv()
+        total = total + plane_recv[0, j].astype(f32)
     out_ref[...] = total.astype(bf16)
 
     def drain(k, carry):
         other = lax.rem(me + k, n)
         small_copy(other, owner).wait_send()
         down_copy(other, owner).wait_send()
-        hits_copy(me, other).wait_send()
+        routes_copy(me, other).wait_send()
         return carry
 
     lax.fori_loop(1, n, drain, 0)
@@ -1176,7 +1239,7 @@
         first_copy(k).wait_send()
         for j in range(1, inner):
             spread_copy(k, j).wait_send()
-            plane_copy(k, j).wait_send()
+            (far_copy if k and j in indirect else plane_copy)(k, j).wait_send()
 
 
 def routed_shards(n, inner, arrays):
@@ -1198,7 +1261,7 @@
     anywhere = pl.BlockSpec(memory_space=pltpu.HBM)
     dma = pltpu.SemaphoreType.DMA
     small_inputs = [pltpu.VMEM(a.shape, a.dtype) for a in arrays[:15]]
-    return pl.pallas_call(
+    results = pl.pallas_call(
         functools.partial(routed_layer, n, inner),
         out_shape=(
             jax.ShapeDtypeStruct((rows, half), bf16),
@@ -1217,10 +1280,12 @@
             pltpu.VMEM((rows, local_heads, head_dim), f32),
             pltpu.VMEM((rows, local_heads, cache_len), f32),
             pltpu.VMEM((rows, local_heads, head_dim), f32),
+            pltpu.VMEM((2, rows * local_heads // 2, cache_len), bf16),
             pltpu.VMEM((rows, model), bf16),
             pltpu.VMEM((n, 2 * units, width), bf16),
             pltpu.VMEM((lanes, half), bf16),
-            pltpu.VMEM((n, rows, lanes), bf16),
+            pltpu.VMEM((n, 1, lanes), f32),
+            pltpu.VMEM((n, rows, lanes), f32),
             pltpu.VMEM((2, rows, half), bf16),
             pltpu.VMEM((2, rows, half), bf16),
             pltpu.VMEM((2, rows, half), bf16),
@@ -1229,11 +1294,12 @@
             pltpu.VMEM((outer, chunk, 4 * hidden + lanes), f32),
             pltpu.VMEM((outer, inner, rows, half), bf16),
             pltpu.VMEM((outer, inner, rows, half), bf16),
+            pltpu.VMEM((outer, inner, rows, half), bf16),
             pltpu.VMEM((outer, rows, half), bf16),
             pltpu.VMEM((outer, rows, half), bf16),
-            dma((18,)),
-            dma((rows // 4,)),
-            dma((rows // 4,)),
+            dma((21,)),
+            dma((2,)),
+            dma((2,)),
             dma((2, 3)),
             dma((2, 2)),
             dma((n,)),
@@ -1245,6 +1311,7 @@
             dma((2, outer, inner)),
             dma((2, outer)),
             dma((2, outer, inner)),
+            dma((2, outer, inner)),
             dma((2, outer)),
         ],
         compiler_params=pltpu.CompilerParams(
@@ -1252,6 +1319,14 @@
         ),
         name="routed_layer",
     )(*[pltpu.with_memory_space_constraint(a, pltpu.HBM) for a in arrays])
+    return pl.pallas_call(
+        finish,
+        out_shape=tuple(jax.ShapeDtypeStruct(r.shape, r.dtype) for r in results),
+        in_specs=[vmem] * 3,
+        out_specs=(anywhere,) * 3,
+        scratch_shapes=[dma((3,))],
+        name="finish",
+    )(*[pltpu.with_memory_space_constraint(r, pltpu.VMEM) for r in results])
 
 
 def shards(

time: 38.6 us -> 33.5 us (0.87)
  Pallas kernels: 36 us -> 32.7 us
  local copies, waits for them, and re-layouts: 1.8 us -> 0 us
    pallas_call x1, Pallas kernels: 36 us -> 32 us  [routed_shards(): pl.pallas_call(functools.partial(routed_layer, n, inner), out_shape=(jax....]
    unnamed x3 -> x0, local copies, waits for them, and re-layouts: 1.8 us -> none
    pallas_call x0 -> x1, Pallas kernels: none -> 0.65 us  [routed_shards(): pl.pallas_call(finish, out_shape=tuple((jax.ShapeDtypeStruct(r.shape, r.d...]
where the time goes in v2:
time: 33.5 us; the launch traced here: 33.3 us
  Pallas kernels  32.7 us (98%)
  between operations  0.65 us (2%)
    pallas_call x1, Pallas kernels, routed_shards(): pl.pallas_call(functools.partial(routed_layer, n, inner), out_shape=(jax....  32 us

profile of v2, /device:TPU:0, one launch (start us, length us, event | category | flops | bytes accessed | tf_op | source)
XLA Modules:
  0.0 33.3 jit_solution(15751940592518227299)
XLA Ops:
  0.6 32.0 %routed_layer.1 = (bf16[16,1024]{1,0:T(8,128)(2,1)S(1)}, bf16[16,64]{1,0:T(8,128)(2,1)S(1)}, bf16[16,64]{1,0:T(8,128)(2,1)S(1)}) custom-call(bf16[16,2048]{1,0:T(8,128)(2,1)} %tokens_hbm.1, f32[1,2048]{1,0:T(1,128)} %bitcast.22, s32[1,16]{1,0:T(1,128)} %bitcast.26, f32[1,8]{1,0:T(1,128)} %bitcast.27, bf16[64,2048]{1,0:T(8,128)(2,1)} %bitcast.19, ...), custom_call_target="tpu_custom_call" | custom-call | tf_op jit(solution)/shard_map/routed_layer/pallas_call | solution.py:1264
  32.7 0.6 %finish.1 = (bf16[16,1024]{1,0:T(8,128)(2,1)}, bf16[16,64]{1,0:T(8,128)(2,1)}, bf16[16,64]{1,0:T(8,128)(2,1)}) custom-call(bf16[16,1024]{1,0:T(8,128)(2,1)S(1)} %get-tuple-element.6.refs_0_, bf16[16,64]{1,0:T(8,128)(2,1)S(1)} %get-tuple-element.7.refs_1_, bf16[16,64]{1,0:T(8,128)(2,1)S(1)} %get-tuple-element.8.refs_2_), custom_call_target="tpu_custom_call" | custom-call | tf_op jit(solution)/shard_map/finish/pallas_call | solution.py:1322

commit v3 on v2

--- a/solution.py
+++ b/solution.py
@@ -685,6 +685,7 @@
     mix_at = router_at + expert_total
     span = rows // 2
     turns = list(range(outer - 1, 0, -1))
+    around = turns[-2:]
     direct = [j for j in range(1, inner) if j & (j - 1) == 0]
     indirect = [j for j in range(1, inner) if j & (j - 1)]
     lines = span * local_heads
@@ -845,6 +846,8 @@
             own_seq = jnp.where(seq_of == s, mixed[s], own_seq)
         read_ref[c * span : (c + 1) * span] = own_seq.T.reshape(span, local_heads, head_dim)
 
+    for c in range(2):
+        stick_breaking(c)
     pl.semaphore_wait(barrier, 2 * n - 1)
     trades = [
         remote(
@@ -920,7 +923,6 @@
     for c in range(2):
         values_load(c).wait()
     for c in range(2):
-        stick_breaking(c)
         read_values(c)
     heads_out = jnp.concatenate([read_ref[:, h, :] for h in range(local_heads)], axis=1).astype(
         bf16
@@ -978,17 +980,28 @@
             core,
         )
 
+    def around_copy(k, j):
+        origin = z * inner + flip(p, j)
+        return remote(
+            norm_all.at[origin],
+            norm_all.at[origin],
+            spread_sems.at[0, k, j],
+            spread_sems.at[1, k, j],
+            flip(z, k) * inner + p,
+            core,
+        )
+
     for k in turns:
         line_copy(k).start()
     for j in indirect + direct:
         spread_copy(0, j).start()
 
+
     lax.fori_loop(1, n, send_down, 0)
 
     @pl.when(owner != core)
     def _():
         down_copy(me, peer).start()
-
 
     across = (((1,), (1,)), ((), ()))
     arrived(w_key_ref, w_value_ref)
@@ -1063,8 +1076,13 @@
 
     for k in turns:
         line_copy(k).wait_recv()
-        for j in indirect + direct:
+        for j in direct if k in around else indirect + direct:
             spread_copy(k, j).start()
+        if k == turns[0]:
+            for j in indirect:
+                spread_copy(0, j).wait_recv()
+                for m in around:
+                    around_copy(m, j).start()
     take_all(small_taken)
 
     arrived(*[target for _, target in pairs[18:]])
@@ -1085,16 +1103,21 @@
     def group(k):
         return pl.ds(pl.multiple_of(flip(z, k) * inner, inner), inner)
 
-    def first(k):
-        for j in range(1, inner):
-            spread_copy(k, j).wait_recv()
-        x = norm_all[group(k)].reshape(chunk, half)
-        first_send[k, :, : 2 * hidden] = jnp.dot(x, w_gate[...], preferred_element_type=f32)
-        first_send[k, :, 2 * hidden : rest_at] = lax.dot_general(
-            x, small[...], across, preferred_element_type=f32
-        )
-        first_send[k, :, rest_at:] = jnp.dot(x, w_up[...], preferred_element_type=f32)
-        first_copy(k).start()
+    def first(*ks):
+        for k in ks:
+            for j in range(1, inner) if k else direct:
+                spread_copy(k, j).wait_recv()
+        x = jnp.concatenate([norm_all[group(k)].reshape(chunk, half) for k in ks], axis=0)
+        gate_rows = jnp.dot(x, w_gate[...], preferred_element_type=f32)
+        rest = lax.dot_general(x, small[...], across, preferred_element_type=f32)
+        up_rows = jnp.dot(x, w_up[...], preferred_element_type=f32)
+        for i, k in enumerate(ks):
+            own_rows = slice(i * chunk, (i + 1) * chunk)
+            first_send[k, :, : 2 * hidden] = gate_rows[own_rows]
+            first_send[k, :, 2 * hidden : rest_at] = rest[own_rows]
+            first_send[k, :, rest_at:] = up_rows[own_rows]
+        for k in ks:
+            first_copy(k).start()
 
     def plane_copy(k, j):
         other = flip(p, j)
@@ -1118,14 +1141,15 @@
         )
 
     def send_plane(k):
+        for j in indirect:
+            if k in turns[:-1]:
+                far_copy(k, j).start()
+            elif k:
+                plane_copy(k, j).start()
         for j in direct:
             plane_copy(k, j).start()
-        if k:
-            for j in indirect:
-                far_copy(k, j).start()
-
-    def second(k):
-        first_copy(k).wait_recv()
+
+    def activations(k):
         gate_rows = first_send[k, :, : 2 * hidden] + first_recv[k, :, : 2 * hidden]
         up_rows = first_send[k, :, rest_at:] + first_recv[k, :, rest_at:]
         rest = first_send[k, :, 2 * hidden : rest_at] + first_recv[k, :, 2 * hidden : rest_at]
@@ -1138,12 +1162,22 @@
         mix_gate = jax.nn.sigmoid(mix_sum)
         dense = jax.nn.silu(rest) * pltpu.roll(rest, lanes - units, 1) * mix_gate
         dense = jnp.where(dense_lane, dense, 0.0).astype(bf16)
-        act = (jax.nn.silu(gate_rows) * up_rows * gate).astype(bf16)
+        return (jax.nn.silu(gate_rows) * up_rows * gate).astype(bf16), dense
+
+    def second(*ks):
+        for k in ks:
+            first_copy(k).wait_recv()
+        parts = [activations(k) for k in ks]
+        act = jnp.concatenate([part[0] for part in parts], axis=0)
+        dense = jnp.concatenate([part[1] for part in parts], axis=0)
         value = jnp.dot(act, w_down[: 2 * hidden], preferred_element_type=f32) + jnp.dot(
             dense, w_down[2 * hidden :], preferred_element_type=f32
         )
-        plane_send[k] = value.astype(bf16).reshape(inner, rows, half)
-        send_plane(k)
+        for i, k in enumerate(ks):
+            own_rows = value[i * chunk : (i + 1) * chunk]
+            plane_send[k] = own_rows.astype(bf16).reshape(inner, rows, half)
+        for k in ks:
+            send_plane(k)
 
     def far_home(j):
         return remote(
@@ -1167,7 +1201,7 @@
 
     def collect(k):
         total = plane_send[k, p].astype(f32)
-        for j in direct:
+        for j in direct + (indirect if k == turns[-1] else []):
             plane_copy(k, j).wait_recv()
             total = total + plane_recv[k, j].astype(f32)
         return total
@@ -1190,23 +1224,24 @@
             hit = jnp.where(named[c * rows : (c + 1) * rows, j : j + 1] == row_lane, 1.0, hit)
         hits_ref[j] = hit
 
-    first(turns[0])
     take_all(down_taken)
     second(0)
-    for before, k in zip(turns, turns[1:]):
+    first(turns[0])
+    for k in turns[1:]:
         first(k)
-        second(before)
-    second(turns[-1])
     for k in turns:
+        second(k)
+    for k in turns[:-1]:
         third(k)
     for j in indirect:
         other = flip(p, j)
         total = plane_send[0, other].astype(f32)
-        for k in turns:
+        for k in turns[:-1]:
             far_copy(k, j).wait_recv()
             total = total + far_recv[k, j].astype(f32)
         far_recv[0, j] = total.astype(bf16)
         far_home(j).start()
+    third(turns[-1])
     total = res_ref[core].astype(f32) + collect(0)
     for k in turns:
         back_copy(k).wait_recv()
@@ -1238,8 +1273,8 @@
             back_copy(k).wait_send()
         first_copy(k).wait_send()
         for j in range(1, inner):
-            spread_copy(k, j).wait_send()
-            (far_copy if k and j in indirect else plane_copy)(k, j).wait_send()
+            (around_copy if k in around and j in indirect else spread_copy)(k, j).wait_send()
+            (far_copy if k in turns[:-1] and j in indirect else plane_copy)(k, j).wait_send()
 
 
 def routed_shards(n, inner, arrays):

time: 33.5 us -> 32.4 us (0.967)
  Pallas kernels: 32.7 us -> 31.6 us
    pallas_call x1, Pallas kernels: 32 us -> 30.9 us  [routed_shards(): pl.pallas_call(functools.partial(routed_layer, n, inner), out_shape=(jax....]
where the time goes in v3:
time: 32.4 us; the launch traced here: 32.2 us
  Pallas kernels  31.6 us (98%)
  between operations  0.65 us (2%)
    pallas_call x1, Pallas kernels, routed_shards(): pl.pallas_call(functools.partial(routed_layer, n, inner), out_shape=(jax....  30.9 us

profile of v3, /device:TPU:0, one launch (start us, length us, event | category | flops | bytes accessed | tf_op | source)
XLA Modules:
  0.0 32.2 jit_solution(17009458812843563327)
XLA Ops:
  0.6 30.9 %routed_layer.1 = (bf16[16,1024]{1,0:T(8,128)(2,1)S(1)}, bf16[16,64]{1,0:T(8,128)(2,1)S(1)}, bf16[16,64]{1,0:T(8,128)(2,1)S(1)}) custom-call(bf16[16,2048]{1,0:T(8,128)(2,1)} %tokens_hbm.1, f32[1,2048]{1,0:T(1,128)} %bitcast.22, s32[1,16]{1,0:T(1,128)} %bitcast.26, f32[1,8]{1,0:T(1,128)} %bitcast.27, bf16[64,2048]{1,0:T(8,128)(2,1)} %bitcast.19, ...), custom_call_target="tpu_custom_call" | custom-call | tf_op jit(solution)/shard_map/routed_layer/pallas_call | solution.py:1299
  31.6 0.6 %finish.1 = (bf16[16,1024]{1,0:T(8,128)(2,1)}, bf16[16,64]{1,0:T(8,128)(2,1)}, bf16[16,64]{1,0:T(8,128)(2,1)}) custom-call(bf16[16,1024]{1,0:T(8,128)(2,1)S(1)} %get-tuple-element.6.refs_0_, bf16[16,64]{1,0:T(8,128)(2,1)S(1)} %get-tuple-element.7.refs_1_, bf16[16,64]{1,0:T(8,128)(2,1)S(1)} %get-tuple-element.8.refs_2_), custom_call_target="tpu_custom_call" | custom-call | tf_op jit(solution)/shard_map/finish/pallas_call | solution.py:1357

commit v4 on v3

--- a/solution.py
+++ b/solution.py
@@ -686,6 +686,7 @@
     span = rows // 2
     turns = list(range(outer - 1, 0, -1))
     around = turns[-2:]
+    homeward = turns[:-1]
     direct = [j for j in range(1, inner) if j & (j - 1) == 0]
     indirect = [j for j in range(1, inner) if j & (j - 1)]
     lines = span * local_heads
@@ -1142,7 +1143,7 @@
 
     def send_plane(k):
         for j in indirect:
-            if k in turns[:-1]:
+            if k in homeward:
                 far_copy(k, j).start()
             elif k:
                 plane_copy(k, j).start()
@@ -1177,7 +1178,8 @@
             own_rows = value[i * chunk : (i + 1) * chunk]
             plane_send[k] = own_rows.astype(bf16).reshape(inner, rows, half)
         for k in ks:
-            send_plane(k)
+            if k:
+                send_plane(k)
 
     def far_home(j):
         return remote(
@@ -1201,7 +1203,7 @@
 
     def collect(k):
         total = plane_send[k, p].astype(f32)
-        for j in direct + (indirect if k == turns[-1] else []):
+        for j in direct + (indirect if k and k not in homeward else []):
             plane_copy(k, j).wait_recv()
             total = total + plane_recv[k, j].astype(f32)
         return total
@@ -1231,17 +1233,41 @@
         first(k)
     for k in turns:
         second(k)
+    send_plane(0)
     for k in turns[:-1]:
         third(k)
     for j in indirect:
         other = flip(p, j)
         total = plane_send[0, other].astype(f32)
-        for k in turns[:-1]:
+        for k in homeward:
             far_copy(k, j).wait_recv()
             total = total + far_recv[k, j].astype(f32)
         far_recv[0, j] = total.astype(bf16)
         far_home(j).start()
     third(turns[-1])
+    def drain(k, carry):
+        other = lax.rem(me + k, n)
+        routes_copy(me, other).wait_send()
+        small_copy(other, owner).wait_send()
+        down_copy(other, owner).wait_send()
+        return carry
+
+    lax.fori_loop(1, n, drain, 0)
+
+    @pl.when(owner != core)
+    def _():
+        small_copy(me, peer).wait_send()
+        down_copy(me, peer).wait_send()
+
+    for copy in trades + swaps:
+        copy.wait_send()
+    for k in range(outer):
+        if k:
+            line_copy(k).wait_send()
+        first_copy(k).wait_send()
+        for j in range(1, inner):
+            (around_copy if k in around and j in indirect else spread_copy)(k, j).wait_send()
+
     total = res_ref[core].astype(f32) + collect(0)
     for k in turns:
         back_copy(k).wait_recv()
@@ -1251,30 +1277,14 @@
         total = total + plane_recv[0, j].astype(f32)
     out_ref[...] = total.astype(bf16)
 
-    def drain(k, carry):
-        other = lax.rem(me + k, n)
-        small_copy(other, owner).wait_send()
-        down_copy(other, owner).wait_send()
-        routes_copy(me, other).wait_send()
-        return carry
-
-    lax.fori_loop(1, n, drain, 0)
-
-    @pl.when(owner != core)
-    def _():
-        small_copy(me, peer).wait_send()
-        down_copy(me, peer).wait_send()
-
-    for copy in trades + swaps:
-        copy.wait_send()
     for k in range(outer):
         if k:
-            line_copy(k).wait_send()
             back_copy(k).wait_send()
-        first_copy(k).wait_send()
         for j in range(1, inner):
-            (around_copy if k in around and j in indirect else spread_copy)(k, j).wait_send()
-            (far_copy if k in turns[:-1] and j in indirect else plane_copy)(k, j).wait_send()
+            if k == 0 and j in indirect:
+                far_home(j).wait_send()
+            else:
+                (far_copy if k in homeward and j in indirect else plane_copy)(k, j).wait_send()
 
 
 def routed_shards(n, inner, arrays):

time: 32.4 us -> 32.2 us (level)
  no operation moved by 1% of the time
where the time goes in v4:
time: 32.2 us; the launch traced here: 32 us
  Pallas kernels  31.4 us (98%)
  between operations  0.65 us (2%)
    pallas_call x1, Pallas kernels, routed_shards(): pl.pallas_call(functools.partial(routed_layer, n, inner), out_shape=(jax....  30.7 us
    pallas_call x1, Pallas kernels, routed_shards(): pl.pallas_call(finish, out_shape=tuple((jax.ShapeDtypeStruct(r.shape, r.d...  0.65 us

profile of v4, /device:TPU:0, one launch (start us, length us, event | category | flops | bytes accessed | tf_op | source)
XLA Modules:
  0.0 32.0 jit_solution(8248246337448045240)
XLA Ops:
  0.6 30.7 %routed_layer.1 = (bf16[16,1024]{1,0:T(8,128)(2,1)S(1)}, bf16[16,64]{1,0:T(8,128)(2,1)S(1)}, bf16[16,64]{1,0:T(8,128)(2,1)S(1)}) custom-call(bf16[16,2048]{1,0:T(8,128)(2,1)} %tokens_hbm.1, f32[1,2048]{1,0:T(1,128)} %bitcast.22, s32[1,16]{1,0:T(1,128)} %bitcast.26, f32[1,8]{1,0:T(1,128)} %bitcast.27, bf16[64,2048]{1,0:T(8,128)(2,1)} %bitcast.19, ...), custom_call_target="tpu_custom_call" | custom-call | tf_op jit(solution)/shard_map/routed_layer/pallas_call | solution.py:1309
  31.4 0.6 %finish.1 = (bf16[16,1024]{1,0:T(8,128)(2,1)}, bf16[16,64]{1,0:T(8,128)(2,1)}, bf16[16,64]{1,0:T(8,128)(2,1)}) custom-call(bf16[16,1024]{1,0:T(8,128)(2,1)S(1)} %get-tuple-element.6.refs_0_, bf16[16,64]{1,0:T(8,128)(2,1)S(1)} %get-tuple-element.7.refs_1_, bf16[16,64]{1,0:T(8,128)(2,1)S(1)} %get-tuple-element.8.refs_2_), custom_call_target="tpu_custom_call" | custom-call | tf_op jit(solution)/shard_map/finish/pallas_call | solution.py:1367

commit v5 on v4

--- a/solution.py
+++ b/solution.py
@@ -686,7 +686,7 @@
     span = rows // 2
     turns = list(range(outer - 1, 0, -1))
     around = turns[-2:]
-    homeward = turns[:-1]
+    homeward = turns
     direct = [j for j in range(1, inner) if j & (j - 1) == 0]
     indirect = [j for j in range(1, inner) if j & (j - 1)]
     lines = span * local_heads
@@ -744,7 +744,7 @@
         block = pl.ds(c * span, span)
         return pltpu.make_async_copy(values_hbm.at[block], values.at[block], values_sem.at[c])
 
-    for load in loads[:12]:
+    for load in loads[:2] + loads[5:9]:
         load.start()
 
     barrier = pltpu.get_barrier_semaphore()
@@ -757,6 +757,8 @@
 
     lax.fori_loop(1, n, greet, 0)
     pl.semaphore_signal(barrier, inc=1, device_id=(me, peer), device_id_type=MESH)
+    for load in loads[2:5] + loads[9:12]:
+        load.start()
 
     arrived(tokens_ref, attn_gain_ref)
     start = tokens_ref[...].astype(f32)

time: 32.2 us -> 32.2 us (level)
  no operation moved by 1% of the time
where the time goes in v5:
time: 32.2 us; the launch traced here: 32.1 us
  Pallas kernels  31.4 us (98%)
  between operations  0.65 us (2%)
    pallas_call x1, Pallas kernels, routed_shards(): pl.pallas_call(functools.partial(routed_layer, n, inner), out_shape=(jax....  30.8 us
    pallas_call x1, Pallas kernels, routed_shards(): pl.pallas_call(finish, out_shape=tuple((jax.ShapeDtypeStruct(r.shape, r.d...  0.65 us

profile of v5, /device:TPU:0, one launch (start us, length us, event | category | flops | bytes accessed | tf_op | source)
XLA Modules:
  0.0 32.1 jit_solution(16022417017660879603)
XLA Ops:
  0.6 30.8 %routed_layer.1 = (bf16[16,1024]{1,0:T(8,128)(2,1)S(1)}, bf16[16,64]{1,0:T(8,128)(2,1)S(1)}, bf16[16,64]{1,0:T(8,128)(2,1)S(1)}) custom-call(bf16[16,2048]{1,0:T(8,128)(2,1)} %tokens_hbm.1, f32[1,2048]{1,0:T(1,128)} %bitcast.22, s32[1,16]{1,0:T(1,128)} %bitcast.26, f32[1,8]{1,0:T(1,128)} %bitcast.27, bf16[64,2048]{1,0:T(8,128)(2,1)} %bitcast.19, ...), custom_call_target="tpu_custom_call" | custom-call | tf_op jit(solution)/shard_map/routed_layer/pallas_call | solution.py:1311
  31.4 0.6 %finish.1 = (bf16[16,1024]{1,0:T(8,128)(2,1)}, bf16[16,64]{1,0:T(8,128)(2,1)}, bf16[16,64]{1,0:T(8,128)(2,1)}) custom-call(bf16[16,1024]{1,0:T(8,128)(2,1)S(1)} %get-tuple-element.6.refs_0_, bf16[16,64]{1,0:T(8,128)(2,1)S(1)} %get-tuple-element.7.refs_1_, bf16[16,64]{1,0:T(8,128)(2,1)S(1)} %get-tuple-element.8.refs_2_), custom_call_target="tpu_custom_call" | custom-call | tf_op jit(solution)/shard_map/finish/pallas_call | solution.py:1369
